TPU v7x, 32 devices: a whole 2x2x4 slice. The times are simulated.
32 devices in a mesh: sp: 8 (over z, core), tp: 4 (over y, x).
Axes of the slice: x: 2, y: 2, z: 4, core: 2. Of those that a mesh axis runs over, the one named last changes fastest.
Arguments:
- residual: bfloat16 [1024, 2048], P('sp', 'tp'), may hold values from -48 to 48
- glu_value: bfloat16 [1024, 2048], P('sp', 'tp'), may hold values from -48 to 48
- glu_gate: bfloat16 [1024, 2048], P('sp', 'tp'), may hold values from -6 to 6
- conv_weight: bfloat16 [31, 2048], P(None, 'tp'), may hold values from -1 to 1
- conv_bias: float32 [2048], P('tp'), may hold values from -3 to 3
- ln_gain: float32 [2048], P('tp'), may hold values from 0.1 to 1.9
- ln_bias: float32 [2048], P('tp'), may hold values from -3 to 3
- out_weight: bfloat16 [2048, 2048], P(None, 'tp'), may hold values from -0.125 to 0.125
- norm_gain: float32 [2048], P('tp'), may hold values from 0.1 to 1.9
- route_ids: int32 [1024, 2], P('sp'), may hold values from 0 to 7, all different within a row; in each aligned block of 128 rows (0 to 127, 128 to 255, ...) at most 64 rows name the same one
- route_weight: float32 [1024, 2], P('sp'), may hold values from 0.1 to 1
- expert_gate: bfloat16 [8, 2048, 4096], P('sp', None, 'tp'), may hold values from -0.125 to 0.125
- expert_up: bfloat16 [8, 2048, 4096], P('sp', None, 'tp'), may hold values from -0.125 to 0.125
- expert_down: bfloat16 [8, 4096, 2048], P('sp', 'tp'), may hold values from -0.09375 to 0.09375
Outputs:
- layer_out: bfloat16 [1024, 2048], P('sp', 'tp')
Inputs may be any that keep to these rules, and one draw needn't show every extreme that they name: `route_ids`: within the 128 rows of one index of sp, no expert is named more than 64 times, and in some such rows one expert is named exactly 64 times.
All inputs are finite; a program needn't handle non-finite values.
Results may differ from a plain program's by a relative error of at most 0.006.
Values may be sent and summed in bfloat16 or wider, within the bound.
A program may use at most 64 MiB of HBM per device.

v0:
```python
import functools

import jax
import jax.numpy as jnp
from jax import lax
from jax.experimental import pallas as pl
from jax.experimental.pallas import tpu as pltpu
from jax.sharding import PartitionSpec as P

TOPK = 2


def with_halo(cells, sides, width):
    for axis, dim in sides:
        count = lax.axis_size(axis)
        ends = count - 1
        head = lax.slice_in_dim(cells, 0, width, axis=dim)
        tail = lax.slice_in_dim(cells, cells.shape[dim] - width, cells.shape[dim], axis=dim)
        cells = jnp.concatenate(
            [
                lax.ppermute(tail, axis, [(i, (i + 1) % count) for i in range(ends)]),
                cells,
                lax.ppermute(head, axis, [((i + 1) % count, i) for i in range(ends)]),
            ],
            axis=dim,
        )
    return cells


def on_device(
    residual,
    glu_value,
    glu_gate,
    conv_weight,
    conv_bias,
    ln_gain,
    ln_bias,
    out_weight,
    norm_gain,
    route_ids,
    route_weight,
    expert_gate,
    expert_up,
    expert_down,
):
    rows = residual.shape[0]
    width_all = out_weight.shape[0]
    gated = (glu_value.astype(jnp.float32) * jax.nn.sigmoid(glu_gate.astype(jnp.float32))).astype(
        jnp.bfloat16
    )
    reach = conv_weight.shape[0] // 2
    padded = with_halo(gated, (("sp", 0),), reach)
    taps = conv_weight.astype(jnp.float32)
    conv = jnp.zeros(gated.shape, jnp.float32) + conv_bias
    for tap in range(conv_weight.shape[0]):
        conv = conv + padded[tap : tap + rows].astype(jnp.float32) * taps[tap]
    totals = lax.psum((jnp.sum(conv, axis=1), jnp.sum(conv * conv, axis=1)), "tp")
    mean = (totals[0] / width_all)[:, None]
    var = (totals[1] / width_all)[:, None] - mean * mean
    act = jax.nn.silu((conv - mean) * lax.rsqrt(var + 1e-05) * ln_gain + ln_bias).astype(
        jnp.bfloat16
    )
    projected = jnp.dot(
        lax.all_gather(act, "tp", axis=1, tiled=True),
        out_weight,
        preferred_element_type=jnp.float32,
    )
    mixed = residual.astype(jnp.float32) + projected
    squares = lax.psum(jnp.sum(mixed * mixed, axis=1), "tp")
    normed = (mixed * lax.rsqrt(squares / width_all + 1e-06)[:, None] * norm_gain).astype(
        jnp.bfloat16
    )
    experts = lax.axis_size("sp")
    capacity = 2 * rows * TOPK // experts
    flat = route_ids.reshape(-1)
    onehot = (flat[:, None] == jnp.arange(experts, dtype=jnp.int32)[None, :]).astype(jnp.int32)
    rank = jnp.sum((jnp.cumsum(onehot, axis=0) - 1) * onehot, axis=1)
    slot_of = flat * capacity + rank
    placing = (slot_of[None, :] == jnp.arange(experts * capacity, dtype=jnp.int32)[:, None]).astype(
        jnp.bfloat16
    )
    copies = jnp.repeat(normed, TOPK, axis=0)
    outgoing = jnp.dot(placing, copies, preferred_element_type=jnp.float32).astype(jnp.bfloat16)
    outgoing = outgoing.reshape(experts, capacity, normed.shape[1])
    arrived = lax.all_to_all(outgoing, "sp", split_axis=0, concat_axis=0, tiled=True)
    arrived = lax.all_gather(
        arrived.reshape(experts * capacity, normed.shape[1]), "tp", axis=1, tiled=True
    )
    gate = jnp.dot(arrived, expert_gate[0], preferred_element_type=jnp.float32)
    up = jnp.dot(arrived, expert_up[0], preferred_element_type=jnp.float32)
    hidden = (jax.nn.silu(gate) * up).astype(jnp.bfloat16)
    partial_out = jnp.dot(hidden, expert_down[0], preferred_element_type=jnp.float32)
    summed = lax.psum_scatter(
        partial_out.astype(jnp.bfloat16), "tp", scatter_dimension=1, tiled=True
    )
    summed = summed.reshape(experts, capacity, summed.shape[1])
    returned = lax.all_to_all(summed, "sp", split_axis=0, concat_axis=0, tiled=True)
    returned = returned.reshape(experts * capacity, returned.shape[2])
    picked = lax.dot_general(
        placing, returned, (((0,), (0,)), ((), ())), preferred_element_type=jnp.float32
    )
    picked = picked.reshape(rows, TOPK, picked.shape[1])
    moe = jnp.sum(picked * route_weight[:, :, None], axis=1)
    return (mixed + moe).astype(jnp.bfloat16)


F32 = jnp.float32
BF16 = jnp.bfloat16
GROUPS = 4


def dot(a, b):
    return jnp.dot(a, b, preferred_element_type=F32)


def layer_kernel(
    nsp, ntp,
    res_hbm, val_hbm, gate_hbm, cw_hbm, cb_hbm, lg_hbm, lb_hbm, ng_hbm, ids_hbm, rw_hbm,
    ow_hbm, eg_hbm, eu_hbm, ed_hbm,
    out_ref,
    res_ref, val_ref, gate_ref, cw_ref, cb_ref, lg_ref, lb_ref, ng_ref, ids_ref, rw_ref,
    ow, wg, wu, wd, pad, wf, conv, mixed, halo_out, halo_in, st_out, st_in,
    act, outgoing, arr, hid, part, one, two_out, two, fin, ret,
    w_sem, halo_s, halo_r, st_s, st_r, ag_s, ag_r, zs_s, zs_r, x_s, x_r, r_s, r_r, h_s, h_r,
):
    rows, ch = res_ref.shape
    width = ow.shape[0]
    taps = cw_ref.shape[0]
    reach = taps // 2
    edge = halo_in.shape[1]
    size = nsp // GROUPS
    cap = outgoing.shape[0] // nsp
    grp = size * cap
    half = grp // 2
    me = lax.axis_index("sp")
    t = lax.axis_index("tp")
    gi, mi = me // size, me % size
    cx, cy = t % 2, t // 2
    tx = cy * 2 + 1 - cx
    ty = (1 - cy) * 2 + cx
    td = (1 - cy) * 2 + 1 - cx

    def remote(src, dst, ss, rs, **dev):
        return pltpu.make_async_remote_copy(
            src_ref=src, dst_ref=dst, send_sem=ss, recv_sem=rs,
            device_id=dev, device_id_type=pl.DeviceIdType.MESH,
        )

    smalls = [
        (val_hbm, val_ref), (gate_hbm, gate_ref), (cw_hbm, cw_ref), (cb_hbm, cb_ref),
        (ids_hbm, ids_ref), (lg_hbm, lg_ref), (lb_hbm, lb_ref), (res_hbm, res_ref),
        (ng_hbm, ng_ref), (rw_hbm, rw_ref),
    ]
    staged = [pltpu.make_async_copy(a, b, w_sem.at[4 + n]) for n, (a, b) in enumerate(smalls)]
    for load in staged:
        load.start()
    barrier = pltpu.get_barrier_semaphore()
    for d in range(1, ntp):
        pl.semaphore_signal(barrier, inc=1, device_id={"tp": (t + d) % ntp},
                            device_id_type=pl.DeviceIdType.MESH)
    for d in range(1, nsp):
        pl.semaphore_signal(barrier, inc=1, device_id={"sp": (me + d) % nsp},
                            device_id_type=pl.DeviceIdType.MESH)
    loads = [
        pltpu.make_async_copy(ow_hbm, ow, w_sem.at[0]),
        pltpu.make_async_copy(eg_hbm.at[0], wg, w_sem.at[1]),
        pltpu.make_async_copy(eu_hbm.at[0], wu, w_sem.at[2]),
        pltpu.make_async_copy(ed_hbm.at[0], wd, w_sem.at[3]),
    ]
    for load in loads:
        load.start()

    staged[0].wait()
    staged[1].wait()
    gated = (val_ref[...].astype(F32) * jax.nn.sigmoid(gate_ref[...].astype(F32))).astype(BF16)
    halo_out[0] = gated[rows - edge:]
    halo_out[1] = gated[:edge]
    pad[edge:edge + rows, :] = gated.astype(F32)
    pad[0:edge, :] = jnp.zeros((edge, ch), F32)
    pad[edge + rows:, :] = jnp.zeros((edge, ch), F32)
    staged[2].wait()
    wf[0:taps, :] = cw_ref[...].astype(F32)
    pl.semaphore_wait(barrier, ntp + nsp - 2)
    to_right = remote(halo_out.at[0], halo_in.at[0], halo_s.at[0], halo_r.at[0], sp=(me + 1) % nsp)
    to_left = remote(halo_out.at[1], halo_in.at[1], halo_s.at[1], halo_r.at[1],
                     sp=(me + nsp - 1) % nsp)

    @pl.when(me < nsp - 1)
    def _():
        to_right.start()

    @pl.when(me > 0)
    def _():
        to_left.start()

    lane = lax.broadcasted_iota(jnp.int32, (rows, 128), 1)
    row = lax.broadcasted_iota(jnp.int32, (rows, rows), 0)
    col = lax.broadcasted_iota(jnp.int32, (rows, rows), 1)
    for load in staged[3:]:
        load.wait()
    topk = ids_ref.shape[0]

    def upright(pair):
        return jnp.concatenate([pair, jnp.zeros((128 - topk, rows), F32)], axis=0).T

    ids = upright(ids_ref[...].astype(F32)).astype(jnp.int32)
    id0, id1 = ids[:, 0:1], ids[:, 1:2]
    weights = upright(rw_ref[...])
    hit0, hit1 = lane == id0, lane == id1
    named = jnp.where(hit0, 1.0, jnp.where(hit1, 1.0, 0.0)).astype(BF16)
    before = jnp.where(col < row, 1.0, 0.0).astype(BF16)
    rank = dot(before, named)
    rank0 = jnp.sum(jnp.where(hit0, rank, 0.0), axis=1, keepdims=True).astype(jnp.int32)
    rank1 = jnp.sum(jnp.where(hit1, rank, 0.0), axis=1, keepdims=True).astype(jnp.int32)
    slot = lax.broadcasted_iota(jnp.int32, (rows, nsp * cap), 1)
    pick0 = jnp.where(slot == id0 * cap + rank0, 1.0, 0.0)
    pick1 = jnp.where(slot == id1 * cap + rank1, 1.0, 0.0)
    placing = (pick0 + pick1).T.astype(BF16)
    pick0 = pick0.astype(BF16)
    pick1 = pick1.astype(BF16)

    @pl.when(me > 0)
    def _():
        to_right.wait_recv()
        pad[0:edge, :] = halo_in[0].astype(F32)

    @pl.when(me < nsp - 1)
    def _():
        to_left.wait_recv()
        pad[edge + rows:, :] = halo_in[1].astype(F32)

    for j in range(0, ch, 128):
        total = jnp.zeros((rows, 128), F32) + cb_ref[:, j:j + 128]
        for tap in range(taps):
            at = tap + edge - reach
            total = total + pad[at:at + rows, j:j + 128] * wf[tap:tap + 1, j:j + 128]
        conv[:, j:j + 128] = total

    def row_totals(which, sums):
        block = jnp.zeros((rows, 128), F32)
        for n, s in enumerate(sums):
            block = jnp.where(lane == n, s, block)
        mine = block.T[0:8, :]
        st_out[which] = mine
        copies = []
        for d in range(1, ntp):
            n = which * ntp + d
            copy = remote(st_out.at[which], st_in.at[which, d], st_s.at[n], st_r.at[n],
                          tp=(t + d) % ntp)
            copy.start()
            copies.append(copy)
        total = mine
        for d, copy in enumerate(copies):
            copy.wait_recv()
            total = total + st_in[which, d + 1]
        back = jnp.concatenate([total, jnp.zeros((rows - 8, 128), F32)], axis=0).T
        return [back[:, n:n + 1] for n in range(len(sums))], copies

    c = conv[...]
    (s1, s2), st1 = row_totals(
        0, (jnp.sum(c, axis=1, keepdims=True), jnp.sum(c * c, axis=1, keepdims=True))
    )
    mean = s1 / width
    var = s2 / width - mean * mean
    act[t] = jax.nn.silu(
        (conv[...] - mean) * lax.rsqrt(var + 1e-05) * lg_ref[...] + lb_ref[...]
    ).astype(BF16)

    mid = rows // 2
    low, high = pl.ds(0, mid), pl.ds(mid, mid)
    ag = [
        remote(act.at[of, at], act.at[of, at], ag_s.at[n], ag_r.at[n], tp=to)
        for n, (of, at, to) in enumerate((
            (t, low, tx), (t, high, ty), (t, high, tx), (t, low, ty), (tx, low, ty), (ty, high, tx),
        ))
    ]

    def arrival(n, block):
        return remote(block, block, ag_s.at[n], ag_r.at[n], tp=tx)

    def columns(of):
        return ow[pl.ds(pl.multiple_of(of * ch, ch), ch), :]

    for n in range(4):
        ag[n].start()
    loads[0].wait()
    mixed[...] = res_ref[...].astype(F32) + dot(act[t], columns(t))
    arrival(0, act.at[tx, low]).wait_recv()
    ag[4].start()
    arrival(1, act.at[ty, high]).wait_recv()
    ag[5].start()
    arrival(2, act.at[tx, high]).wait_recv()
    arrival(3, act.at[ty, low]).wait_recv()
    mixed[...] += dot(act[tx], columns(tx)) + dot(act[ty], columns(ty))
    arrival(4, act.at[td, low]).wait_recv()
    arrival(5, act.at[td, high]).wait_recv()
    full = mixed[...] + dot(act[td], columns(td))
    mixed[...] = full
    (sq,), st2 = row_totals(1, (jnp.sum(full * full, axis=1, keepdims=True),))
    normed = (mixed[...] * lax.rsqrt(sq / width + 1e-06) * ng_ref[...]).astype(BF16)
    outgoing[...] = dot(placing, normed).astype(BF16)

    def piece(n):
        return pl.ds(pl.multiple_of(n * cap, cap), cap)

    zs = []
    for k in range(GROUPS):
        for i in range(size):
            if k == 0 and i == 0:
                continue
            e = (gi - k + GROUPS) % GROUPS * size + (mi + i) % size
            place = k * size + mi
            copy = remote(outgoing.at[piece(e)], arr.at[t, piece(place)],
                          zs_s.at[k * size + i], zs_r.at[place], sp=e)
            copy.start()
            zs.append(copy)
    arr[t, piece(mi), :] = outgoing[piece(me), :]

    pending = []

    def send(copy):
        copy.start()
        pending.append(copy)

    def span(k):
        return pl.ds(k * grp, grp)

    def front(k):
        return pl.ds(k * grp, half)

    def rear(k):
        return pl.ds(k * grp + half, half)

    def share(k):
        for i in range(size):
            if k == 0 and i == 0:
                continue
            place = k * size + (mi + i) % size
            remote(outgoing.at[piece(0)], arr.at[t, piece(place)], zs_s.at[0], zs_r.at[place],
                   sp=me).wait_recv()
        pass_on(k, 0, t, front(k), tx)
        pass_on(k, 1, t, rear(k), ty)
        pass_on(k, 2, t, rear(k), tx)
        pass_on(k, 3, t, front(k), ty)

    def pass_on(k, n, of, at, to):
        block = arr.at[of, at]
        send(remote(block, block, x_s.at[6 * k + n], x_r.at[6 * k + n], tp=to))

    def landed(k, n, of, at):
        block = arr.at[of, at]
        remote(block, block, x_s.at[6 * k + n], x_r.at[6 * k + n], tp=tx).wait_recv()

    def relay(k):
        landed(k, 0, tx, front(k))
        pass_on(k, 4, tx, front(k), ty)
        landed(k, 1, ty, rear(k))
        pass_on(k, 5, ty, rear(k), tx)

    def gather_end(k):
        landed(k, 2, tx, rear(k))
        landed(k, 3, ty, front(k))
        landed(k, 4, td, front(k))
        landed(k, 5, td, rear(k))

    inner = wg.shape[1]
    tile = min(256, inner)

    def expert_up(k):
        def up(n, carry):
            at = pl.ds(pl.multiple_of(n * tile, tile), tile)
            g = jnp.zeros((grp, tile), F32)
            u = jnp.zeros((grp, tile), F32)
            for b in range(ntp):
                x = arr[b, k * grp:(k + 1) * grp, :]
                g = g + dot(x, wg[b * ch:(b + 1) * ch, at])
                u = u + dot(x, wu[b * ch:(b + 1) * ch, at])
            hid[:, at] = (jax.nn.silu(g) * u).astype(BF16)
            return carry

        if k == 0:
            loads[1].wait()
            loads[2].wait()
        lax.fori_loop(0, inner // tile, up, 0)

    def expert_down(k):
        def down(b, carry):
            at = pl.ds(pl.multiple_of(b * ch, ch), ch)
            part[b, k * grp:(k + 1) * grp, :] = dot(hid[...], wd[:, at]).astype(BF16)
            return carry

        if k == 0:
            loads[3].wait()
        lax.fori_loop(0, ntp, down, 0)
        n = 6 * k
        first = [
            (part.at[tx, front(k)], one.at[0, front(k)], n, tx),
            (part.at[td, front(k)], one.at[1, front(k)], n + 1, tx),
            (part.at[ty, rear(k)], one.at[0, rear(k)], n + 2, ty),
            (part.at[td, rear(k)], one.at[1, rear(k)], n + 3, ty),
        ]
        for src, dst, m, to in (first[1], first[3], first[0], first[2]):
            send(remote(src, dst, r_s.at[m], r_r.at[m], tp=to))

    def summed(m, block):
        remote(block, block, r_s.at[m], r_r.at[m], tp=tx).wait_recv()

    def reduce_mid(k):
        n = 6 * k
        for m, at, to in ((n + 1, front(k), ty), (n + 3, rear(k), tx)):
            summed(m, one.at[1, at])
            two_out[at, :] = (part[to, at, :].astype(F32) + one[1, at, :].astype(F32)).astype(BF16)
            m2 = n + 4 + (m - n) // 2
            send(remote(two_out.at[at], two.at[at], r_s.at[m2], r_r.at[m2], tp=to))

    def reduce_end(k):
        n = 6 * k
        summed(n, one.at[0, front(k)])
        summed(n + 2, one.at[0, rear(k)])
        summed(n + 4, two.at[front(k)])
        summed(n + 5, two.at[rear(k)])
        at = span(k)
        fin[at, :] = (
            part[t, at, :].astype(F32) + one[0, at, :].astype(F32) + two[at, :].astype(F32)
        ).astype(BF16)
        for i in range(size):
            if k == 0 and i == 0:
                ret[piece(me), :] = fin[piece(mi), :]
                continue
            who = (mi + i) % size
            home = (gi + k) % GROUPS * size + who
            send(remote(fin.at[piece(k * size + who)], ret.at[piece(me)],
                        h_s.at[k * size + i], h_r.at[me], sp=home))

    order = [(share, 0), (relay, 0), (share, 1)]
    for k in range(GROUPS):
        order += [(gather_end, k), (expert_up, k)]
        if k >= 1:
            order += [(reduce_mid, k - 1)]
        if k + 1 < GROUPS:
            order += [(relay, k + 1)]
        order += [(expert_down, k)]
        if k + 2 < GROUPS:
            order += [(share, k + 2)]
        if k >= 1:
            order += [(reduce_end, k - 1)]
    order += [(reduce_mid, GROUPS - 1), (reduce_end, GROUPS - 1)]
    for step, k in order:
        step(k)

    for d in range(1, nsp):
        e = (me + d) % nsp
        remote(fin.at[piece(0)], ret.at[piece(e)], h_s.at[0], h_r.at[e], sp=me).wait_recv()
    back = ret[...]
    moe = dot(pick0, back) * weights[:, 0:1] + dot(pick1, back) * weights[:, 1:2]
    out_ref[...] = (mixed[...] + moe).astype(out_ref.dtype)

    @pl.when(me < nsp - 1)
    def _():
        to_right.wait_send()

    @pl.when(me > 0)
    def _():
        to_left.wait_send()

    for copy in st1 + st2 + ag + zs + pending:
        copy.wait_send()


def fused(nsp, ntp, *args):
    (residual, glu_value, glu_gate, conv_weight, conv_bias, ln_gain, ln_bias, out_weight,
     norm_gain, route_ids, route_weight, expert_gate, expert_up, expert_down) = args
    rows, ch = residual.shape
    width = out_weight.shape[0]
    inner = expert_gate.shape[2]
    cap = 2 * rows * TOPK // nsp
    slots = nsp * cap
    grp = slots // GROUPS
    edge = -(-(conv_weight.shape[0] // 2) // 16) * 16
    small = [residual, glu_value, glu_gate, conv_weight]
    small += [a.reshape(1, ch) for a in (conv_bias, ln_gain, ln_bias, norm_gain)]
    small += [route_ids.T, route_weight.T]
    vmem = pl.BlockSpec(memory_space=pltpu.VMEM)
    hbm = pl.BlockSpec(memory_space=pl.ANY)
    dma = lambda n: pltpu.SemaphoreType.DMA((n,))
    return pl.pallas_call(
        functools.partial(layer_kernel, nsp, ntp),
        out_shape=jax.ShapeDtypeStruct((rows, ch), residual.dtype),
        in_specs=[hbm] * 14,
        out_specs=vmem,
        scratch_shapes=[pltpu.VMEM(a.shape, a.dtype) for a in small] + [
            pltpu.VMEM((width, ch), BF16),
            pltpu.VMEM((width, inner), BF16),
            pltpu.VMEM((width, inner), BF16),
            pltpu.VMEM((inner, width), BF16),
            pltpu.VMEM((rows + 2 * edge, ch), F32),
            pltpu.VMEM((-(-conv_weight.shape[0] // 8) * 8, ch), F32),
            pltpu.VMEM((rows, ch), F32),
            pltpu.VMEM((rows, ch), F32),
            pltpu.VMEM((2, edge, ch), BF16),
            pltpu.VMEM((2, edge, ch), BF16),
            pltpu.VMEM((2, 8, 128), F32),
            pltpu.VMEM((2, ntp, 8, 128), F32),
            pltpu.VMEM((ntp, rows, ch), BF16),
            pltpu.VMEM((slots, ch), BF16),
            pltpu.VMEM((ntp, slots, ch), BF16),
            pltpu.VMEM((grp, inner), BF16),
            pltpu.VMEM((ntp, slots, ch), BF16),
            pltpu.VMEM((2, slots, ch), BF16),
            pltpu.VMEM((slots, ch), BF16),
            pltpu.VMEM((slots, ch), BF16),
            pltpu.VMEM((slots, ch), BF16),
            pltpu.VMEM((slots, ch), BF16),
            dma(14), dma(2), dma(2), dma(2 * ntp), dma(2 * ntp), dma(6), dma(6),
            dma(nsp), dma(nsp), dma(6 * GROUPS), dma(6 * GROUPS), dma(6 * GROUPS),
            dma(6 * GROUPS), dma(nsp), dma(nsp),
        ],
        compiler_params=pltpu.CompilerParams(
            collective_id=0, has_side_effects=True, vmem_limit_bytes=67043328
        ),
    )(*small, out_weight, expert_gate, expert_up, expert_down)


def solution(mesh):
    in_specs = (
        P("sp", "tp"),
        P("sp", "tp"),
        P("sp", "tp"),
        P(None, "tp"),
        P("tp"),
        P("tp"),
        P("tp"),
        P(None, "tp"),
        P("tp"),
        P("sp", None),
        P("sp", None),
        P("sp", None, "tp"),
        P("sp", None, "tp"),
        P("sp", "tp", None),
    )
    out_specs = P("sp", "tp")
    nsp, ntp = mesh.shape["sp"], mesh.shape["tp"]
    body = on_device
    if ntp == 4 and nsp % GROUPS == 0:
        body = functools.partial(fused, nsp, ntp)
    return jax.shard_map(
        body, mesh=mesh, in_specs=in_specs, out_specs=out_specs, check_vma=False
    )
```

profile of v0, /device:TPU:0, one launch (start us, length us, event | category | flops | bytes accessed | tf_op | source)
XLA Modules:
  0.0 73.3 jit_solution(18441982002566789651)
XLA Ops:
  0.0 71.7 %shard_map.136 = bf16[128,512]{1,0:T(8,128)(2,1)} custom-call(bf16[128,512]{1,0:T(8,128)(2,1)} %res_hbm.1, bf16[128,512]{1,0:T(8,128)(2,1)} %val_hbm.1, bf16[128,512]{1,0:T(8,128)(2,1)} %gate_hbm.1, bf16[31,512]{1,0:T(8,128)(2,1)} %cw_hbm.1, f32[1,512]{1,0:T(1,128)} %bitcast.6, f32[1,512]{1,0:T(1,128)} %bitcast.7, f32[1,512]{1,0:T(1,128)} %bitcast.8, ...), custom_call_target="tpu_custom_call" | custom-call | tf_op jit(solution)/shard_map/pallas_call | solution.py:486
  71.7 1.6 %copy.16 = bf16[128,512]{1,0:T(8,128)(2,1)} copy(bf16[128,512]{1,0:T(8,128)(2,1)} %shard_map.136) | data formatting | bytes 262144
where the time goes:
time: 73.4 us; the launch traced here: 73.3 us
  Pallas kernels  71.7 us (98%)
  local copies, waits for them, and re-layouts  1.57 us (2%)
    pallas_call x1, Pallas kernels, fused(): pl.pallas_call(functools.partial(layer_kernel, nsp, ntp), out_shape=jax.S...  71.7 us
    unnamed x1, local copies, waits for them, and re-layouts  1.57 us

commit v1 on v0

v1 whole, which is shorter than its diff:
```python
import functools

import jax
import jax.numpy as jnp
from jax import lax
from jax.experimental import pallas as pl
from jax.experimental.pallas import tpu as pltpu
from jax.sharding import PartitionSpec as P

TOPK = 2


def with_halo(cells, sides, width):
    for axis, dim in sides:
        count = lax.axis_size(axis)
        ends = count - 1
        head = lax.slice_in_dim(cells, 0, width, axis=dim)
        tail = lax.slice_in_dim(cells, cells.shape[dim] - width, cells.shape[dim], axis=dim)
        cells = jnp.concatenate(
            [
                lax.ppermute(tail, axis, [(i, (i + 1) % count) for i in range(ends)]),
                cells,
                lax.ppermute(head, axis, [((i + 1) % count, i) for i in range(ends)]),
            ],
            axis=dim,
        )
    return cells


def on_device(
    residual,
    glu_value,
    glu_gate,
    conv_weight,
    conv_bias,
    ln_gain,
    ln_bias,
    out_weight,
    norm_gain,
    route_ids,
    route_weight,
    expert_gate,
    expert_up,
    expert_down,
):
    rows = residual.shape[0]
    width_all = out_weight.shape[0]
    gated = (glu_value.astype(jnp.float32) * jax.nn.sigmoid(glu_gate.astype(jnp.float32))).astype(
        jnp.bfloat16
    )
    reach = conv_weight.shape[0] // 2
    padded = with_halo(gated, (("sp", 0),), reach)
    taps = conv_weight.astype(jnp.float32)
    conv = jnp.zeros(gated.shape, jnp.float32) + conv_bias
    for tap in range(conv_weight.shape[0]):
        conv = conv + padded[tap : tap + rows].astype(jnp.float32) * taps[tap]
    totals = lax.psum((jnp.sum(conv, axis=1), jnp.sum(conv * conv, axis=1)), "tp")
    mean = (totals[0] / width_all)[:, None]
    var = (totals[1] / width_all)[:, None] - mean * mean
    act = jax.nn.silu((conv - mean) * lax.rsqrt(var + 1e-05) * ln_gain + ln_bias).astype(
        jnp.bfloat16
    )
    projected = jnp.dot(
        lax.all_gather(act, "tp", axis=1, tiled=True),
        out_weight,
        preferred_element_type=jnp.float32,
    )
    mixed = residual.astype(jnp.float32) + projected
    squares = lax.psum(jnp.sum(mixed * mixed, axis=1), "tp")
    normed = (mixed * lax.rsqrt(squares / width_all + 1e-06)[:, None] * norm_gain).astype(
        jnp.bfloat16
    )
    experts = lax.axis_size("sp")
    capacity = 2 * rows * TOPK // experts
    flat = route_ids.reshape(-1)
    onehot = (flat[:, None] == jnp.arange(experts, dtype=jnp.int32)[None, :]).astype(jnp.int32)
    rank = jnp.sum((jnp.cumsum(onehot, axis=0) - 1) * onehot, axis=1)
    slot_of = flat * capacity + rank
    placing = (slot_of[None, :] == jnp.arange(experts * capacity, dtype=jnp.int32)[:, None]).astype(
        jnp.bfloat16
    )
    copies = jnp.repeat(normed, TOPK, axis=0)
    outgoing = jnp.dot(placing, copies, preferred_element_type=jnp.float32).astype(jnp.bfloat16)
    outgoing = outgoing.reshape(experts, capacity, normed.shape[1])
    arrived = lax.all_to_all(outgoing, "sp", split_axis=0, concat_axis=0, tiled=True)
    arrived = lax.all_gather(
        arrived.reshape(experts * capacity, normed.shape[1]), "tp", axis=1, tiled=True
    )
    gate = jnp.dot(arrived, expert_gate[0], preferred_element_type=jnp.float32)
    up = jnp.dot(arrived, expert_up[0], preferred_element_type=jnp.float32)
    hidden = (jax.nn.silu(gate) * up).astype(jnp.bfloat16)
    partial_out = jnp.dot(hidden, expert_down[0], preferred_element_type=jnp.float32)
    summed = lax.psum_scatter(
        partial_out.astype(jnp.bfloat16), "tp", scatter_dimension=1, tiled=True
    )
    summed = summed.reshape(experts, capacity, summed.shape[1])
    returned = lax.all_to_all(summed, "sp", split_axis=0, concat_axis=0, tiled=True)
    returned = returned.reshape(experts * capacity, returned.shape[2])
    picked = lax.dot_general(
        placing, returned, (((0,), (0,)), ((), ())), preferred_element_type=jnp.float32
    )
    picked = picked.reshape(rows, TOPK, picked.shape[1])
    moe = jnp.sum(picked * route_weight[:, :, None], axis=1)
    return (mixed + moe).astype(jnp.bfloat16)


F32 = jnp.float32
BF16 = jnp.bfloat16
GROUPS = 4
VMEM_LIMIT = 67043328


def dot(a, b):
    return jnp.dot(a, b, preferred_element_type=F32)


def layer_kernel(
    nsp, ntp,
    res_hbm, val_hbm, gate_hbm, cw_hbm, cb_hbm, lg_hbm, lb_hbm, ng_hbm, ids_hbm, rw_hbm,
    ow_hbm, eg_hbm, eu_hbm, ed_hbm,
    out_ref,
    res_ref, val_ref, gate_ref, cw_ref, cb_ref, lg_ref, lb_ref, ng_ref, ids_ref, rw_ref,
    ow, wg, wu, wd, pad, wf, conv, mixed, halo_out, halo_in, st_out, st_in, lg_all, lb_all,
    cc, outgoing, arr, hid, part, one, two_out, two, fin, ret, rs_out, rs_in,
    w_sem, halo_s, halo_r, st_s, st_r, ln_s, ln_r, ag_s, ag_r, zs_s, zs_r, rs_s, rs_r,
    x_s, x_r, r_s, r_r, h_s, h_r,
):
    rows, ch = res_ref.shape
    width = ow.shape[0]
    taps = cw_ref.shape[0]
    reach = taps // 2
    edge = halo_in.shape[1]
    cap = outgoing.shape[0] // nsp
    grp = 2 * cap
    last = GROUPS - 1
    me = lax.axis_index("sp")
    t = lax.axis_index("tp")
    z, mi = me // 2, me % 2
    cx, cy = t % 2, t // 2
    tx = cy * 2 + 1 - cx
    ty = (1 - cy) * 2 + cx
    td = (1 - cy) * 2 + 1 - cx
    far_side = z // 2
    inner = (z + far_side) % 2
    sign = 1 - 2 * far_side
    chips = [
        z,
        far_side * last + sign * (1 + inner),
        far_side * last + sign * last,
        far_side * last + sign * (2 - 2 * inner),
    ]
    sib = 2 * z + 1 - mi

    def remote(src, dst, ss, rs, **dev):
        return pltpu.make_async_remote_copy(
            src_ref=src, dst_ref=dst, send_sem=ss, recv_sem=rs,
            device_id=dev, device_id_type=pl.DeviceIdType.MESH,
        )

    smalls = [
        (val_hbm, val_ref), (gate_hbm, gate_ref), (cw_hbm, cw_ref), (cb_hbm, cb_ref),
        (lg_hbm, lg_ref), (lb_hbm, lb_ref), (ids_hbm, ids_ref), (res_hbm, res_ref),
        (ng_hbm, ng_ref), (rw_hbm, rw_ref),
    ]
    staged = [pltpu.make_async_copy(a, b, w_sem.at[4 + n]) for n, (a, b) in enumerate(smalls)]
    for load in staged:
        load.start()
    barrier = pltpu.get_barrier_semaphore()
    for d in range(1, ntp):
        pl.semaphore_signal(barrier, inc=1, device_id={"tp": (t + d) % ntp},
                            device_id_type=pl.DeviceIdType.MESH)
    for d in range(1, nsp):
        pl.semaphore_signal(barrier, inc=1, device_id={"sp": (me + d) % nsp},
                            device_id_type=pl.DeviceIdType.MESH)
    loads = [
        pltpu.make_async_copy(ow_hbm, ow, w_sem.at[0]),
        pltpu.make_async_copy(eg_hbm.at[0], wg, w_sem.at[1]),
        pltpu.make_async_copy(eu_hbm.at[0], wu, w_sem.at[2]),
        pltpu.make_async_copy(ed_hbm.at[0], wd, w_sem.at[3]),
    ]
    for load in loads:
        load.start()

    with jax.named_scope("glu"):
        staged[0].wait()
        staged[1].wait()
        gated = (val_ref[...].astype(F32) * jax.nn.sigmoid(gate_ref[...].astype(F32))).astype(BF16)
        halo_out[0] = gated[rows - edge:]
        halo_out[1] = gated[:edge]
        pad[edge:edge + rows, :] = gated.astype(F32)
        pad[0:edge, :] = jnp.zeros((edge, ch), F32)
        pad[edge + rows:, :] = jnp.zeros((edge, ch), F32)
        for load in staged[2:6]:
            load.wait()
        wf[0:taps, :] = cw_ref[...].astype(F32)
    with jax.named_scope("bar"):
        pl.semaphore_wait(barrier, ntp + nsp - 2)
    to_right = remote(halo_out.at[0], halo_in.at[0], halo_s.at[0], halo_r.at[0], sp=(me + 1) % nsp)
    to_left = remote(halo_out.at[1], halo_in.at[1], halo_s.at[1], halo_r.at[1],
                     sp=(me + nsp - 1) % nsp)

    @pl.when(me < nsp - 1)
    def _():
        to_right.start()

    @pl.when(me > 0)
    def _():
        to_left.start()

    pending = []

    def send(copy):
        copy.start()
        pending.append(copy)

    others = (tx, ty, td)
    for n, to in enumerate(others):
        send(remote(lg_ref, lg_all.at[t], ln_s.at[n], ln_r.at[t], tp=to))
        send(remote(lb_ref, lb_all.at[t], ln_s.at[ntp + n], ln_r.at[ntp + t], tp=to))

    def convolve(low, high):
        for j in range(0, ch, 128):
            total = jnp.zeros((high - low, 128), F32) + cb_ref[:, j:j + 128]
            for tap in range(taps):
                at = low + tap + edge - reach
                total = total + pad[at:at + high - low, j:j + 128] * wf[tap:tap + 1, j:j + 128]
            conv[low:high, j:j + 128] = total

    with jax.named_scope("conv_mid"):
        convolve(edge, rows - edge)

    with jax.named_scope("halo"):
        @pl.when(me > 0)
        def _():
            to_right.wait_recv()
            pad[0:edge, :] = halo_in[0].astype(F32)

        @pl.when(me < nsp - 1)
        def _():
            to_left.wait_recv()
            pad[edge + rows:, :] = halo_in[1].astype(F32)

    with jax.named_scope("conv_edge"):
        convolve(0, edge)
        convolve(rows - edge, rows)

    lane = lax.broadcasted_iota(jnp.int32, (rows, 128), 1)

    def send_totals(which, sums):
        block = jnp.zeros((rows, 128), F32)
        for n, s in enumerate(sums):
            block = jnp.where(lane == n, s, block)
        st_out[which] = block.T[0:8, :]
        for n, to in enumerate(others):
            k = which * ntp
            send(remote(st_out.at[which], st_in.at[which, t], st_s.at[k + n], st_r.at[k + t],
                        tp=to))

    def totals_of(which, b):
        ref = st_in.at[which, b]
        remote(st_out.at[which], ref, st_s.at[0], st_r.at[which * ntp + b], tp=tx).wait_recv()
        return st_in[which, b]

    def upright(block):
        fill = jnp.zeros((128 - block.shape[0], block.shape[1]), F32)
        return jnp.concatenate([block, fill], axis=0).T

    quart = rows // 4

    def quarter(of, q):
        return cc.at[of, pl.ds(q * quart, quart)]

    with jax.named_scope("center"):
        c = conv[...]
        s1 = jnp.sum(c, axis=1, keepdims=True)
        c = c - s1 / ch
        cc[t] = c.astype(BF16)
        for q in (0, 1, 2, 3):
            block = quarter(t, q)
            send(remote(block, block, ag_s.at[q], ag_r.at[2 * q + q % 2], tp=(tx, ty)[q % 2]))
        send_totals(0, (s1, jnp.sum(c * c, axis=1, keepdims=True)))
        for q in (1, 0, 3, 2):
            block = quarter(t, q)
            send(remote(block, block, ag_s.at[4 + q], ag_r.at[2 * q + 1 - q % 2],
                        tp=(ty, tx)[q % 2]))

    def arrived(of, q, n):
        block = quarter(of, q)
        remote(block, block, ag_s.at[0], ag_r.at[n], tp=tx).wait_recv()

    with jax.named_scope("routes"):
        row = lax.broadcasted_iota(jnp.int32, (rows, rows), 0)
        col = lax.broadcasted_iota(jnp.int32, (rows, rows), 1)
        for load in staged[6:]:
            load.wait()
        ids = upright(ids_ref[...].astype(F32)).astype(jnp.int32)
        id0, id1 = ids[:, 0:1], ids[:, 1:2]
        weights = upright(rw_ref[...])
        hit0, hit1 = lane == id0, lane == id1
        named = jnp.where(hit0, 1.0, jnp.where(hit1, 1.0, 0.0)).astype(BF16)
        before = jnp.where(col < row, 1.0, 0.0).astype(BF16)
        rank = dot(before, named)
        rank0 = jnp.sum(jnp.where(hit0, rank, 0.0), axis=1, keepdims=True).astype(jnp.int32)
        rank1 = jnp.sum(jnp.where(hit1, rank, 0.0), axis=1, keepdims=True).astype(jnp.int32)
        slot = lax.broadcasted_iota(jnp.int32, (rows, nsp * cap), 1)
        pick0 = jnp.where(slot == id0 * cap + rank0, 1.0, 0.0)
        pick1 = jnp.where(slot == id1 * cap + rank1, 1.0, 0.0)
        placing = (pick0 + pick1).T.astype(BF16)
        pick0 = pick0.astype(BF16)
        pick1 = pick1.astype(BF16)
        wide = lax.broadcasted_iota(jnp.int32, (rows, nsp * grp), 1)
        lead0, lead1 = id0 * grp + mi * cap + rank0, id1 * grp + mi * cap + rank1
        pick_r = jnp.where(wide == lead0, 1.0, jnp.where(wide == lead1, 1.0, 0.0)).astype(BF16)

    def relay_ag(q):
        of, n, to = ((tx, 2 * q, ty), (ty, 2 * q + 1, tx))[q % 2]
        arrived(of, q, n)
        block = quarter(of, q)
        send(remote(block, block, ag_s.at[8 + q], ag_r.at[8 + q], tp=to))

    def columns(of):
        return ow[pl.ds(pl.multiple_of(of * ch, ch), ch), :]

    with jax.named_scope("relay_a"):
        relay_ag(0)
        relay_ag(1)
    with jax.named_scope("ln_stats"):
        lg_all[t] = lg_ref[...]
        lb_all[t] = lb_ref[...]
        stats = [st_out[0]] + [totals_of(0, b) for b in others]
        total = stats[0] + stats[1] + stats[2] + stats[3]
        mean = total[0:1] / width
        offs = [s[0:1] / ch - mean for s in stats]
        spread = sum(o * o for o in offs)
        rstd = lax.rsqrt((total[1:2] + ch * spread) / width + 1e-05)
        cols = upright(jnp.concatenate([rstd] + [o * rstd for o in offs], axis=0))
        rstd = cols[:, 0:1]

    def project(of, n):
        a = cc[of].astype(F32) * rstd + cols[:, n:n + 1]
        a = jax.nn.silu(a * lg_all[of] + lb_all[of]).astype(BF16)
        return dot(a, columns(of))

    with jax.named_scope("proj_own"):
        loads[0].wait()
        mixed[...] = res_ref[...].astype(F32) + project(t, 1)
    with jax.named_scope("relay_b"):
        relay_ag(2)
        relay_ag(3)
        for n, b in enumerate(others):
            remote(lg_ref, lg_all.at[b], ln_s.at[0], ln_r.at[b], tp=tx).wait_recv()
            remote(lb_ref, lb_all.at[b], ln_s.at[0], ln_r.at[ntp + b], tp=tx).wait_recv()
    with jax.named_scope("proj_x"):
        arrived(tx, 1, 2)
        arrived(tx, 3, 6)
        mixed[...] += project(tx, 2)
    with jax.named_scope("proj_y"):
        arrived(ty, 0, 1)
        arrived(ty, 2, 5)
        mixed[...] += project(ty, 3)
    with jax.named_scope("proj_d"):
        for q in range(4):
            arrived(td, q, 8 + q)
        full = mixed[...] + project(td, 4)
        mixed[...] = full
    with jax.named_scope("pick"):
        sq = jnp.sum(full * full, axis=1, keepdims=True)
        outgoing[...] = dot(placing, (full * ng_ref[...]).astype(BF16)).astype(BF16)

    def piece(n):
        return pl.ds(pl.multiple_of(n * cap, cap), cap)

    def dispatch(e):
        remote(outgoing.at[piece(e)], arr.at[t, piece(me)], zs_s.at[e], zs_r.at[me], sp=e).start()

    def dispatch_chip(c):
        dispatch(2 * c + mi)
        dispatch(2 * c + 1 - mi)

    def dispatch_pair():
        dispatch_chip(far_side * last + sign * 2)
        dispatch_chip(far_side * last + sign * (3 - 3 * inner))

    with jax.named_scope("zsend"):
        dispatch(sib)

        @pl.when(inner == 1)
        def _():
            dispatch_pair()

        arr[t, piece(me), :] = outgoing[piece(me), :]
        send_totals(1, (sq,))

    def rows_of(k):
        return pl.ds(pl.multiple_of(chips[k] * grp, grp), grp)

    def half(k, c):
        return piece(2 * chips[k] + c)

    def pass_on(k, n, of, at, to):
        block = arr.at[of, at]
        send(remote(block, block, x_s.at[6 * k + n], x_r.at[6 * k + n], tp=to))

    def landed(k, n, of, at):
        block = arr.at[of, at]
        remote(block, block, x_s.at[6 * k + n], x_r.at[6 * k + n], tp=tx).wait_recv()

    def came(e):
        remote(outgoing.at[piece(0)], arr.at[t, piece(e)], zs_s.at[0], zs_r.at[e],
               sp=me).wait_recv()

    def share(k):
        if k == 0:
            pass_on(0, 2 * mi, t, piece(me), tx)
            pass_on(0, 2 * mi + 1, t, piece(me), ty)
            came(sib)
            pass_on(0, 2 * (1 - mi), t, piece(sib), tx)
            pass_on(0, 2 * (1 - mi) + 1, t, piece(sib), ty)
            return
        came(2 * chips[k])
        came(2 * chips[k] + 1)
        pass_on(k, 0, t, half(k, 0), tx)
        pass_on(k, 3, t, half(k, 1), ty)
        pass_on(k, 2, t, half(k, 1), tx)
        pass_on(k, 1, t, half(k, 0), ty)

    def relay(k):
        landed(k, 0, tx, half(k, 0))
        pass_on(k, 4, tx, half(k, 0), ty)
        landed(k, 3, ty, half(k, 1))
        pass_on(k, 5, ty, half(k, 1), tx)

    def gather_end(k):
        landed(k, 1, ty, half(k, 0))
        landed(k, 2, tx, half(k, 1))
        landed(k, 4, td, half(k, 0))
        landed(k, 5, td, half(k, 1))

    def scales(k):
        r = lax.rsqrt((st_out[1] + totals_of(1, tx) + totals_of(1, ty) + totals_of(1, td)) / width
                      + 1e-06)[0:1]
        top = r.astype(BF16).astype(F32)
        mid = (r - top).astype(BF16).astype(F32)
        low = r - top - mid
        three = jnp.concatenate([top, mid, low, jnp.zeros((13, rows), F32)], axis=0).astype(BF16)
        picked = dot(three, pick_r)
        picked = picked[0:1] + picked[1:2] + picked[2:3]
        for e in range(nsp):
            rs_out[e] = jnp.broadcast_to(picked[:, e * grp:(e + 1) * grp], (8, grp))
        for d in range(1, nsp):
            e = (me + d) % nsp
            send(remote(rs_out.at[e], rs_in.at[me], rs_s.at[e], rs_r.at[me], sp=e))
        rs_in[me] = rs_out[me]

        @pl.when(inner == 0)
        def _():
            dispatch_pair()

    def dispatch_last(k):
        dispatch_chip(far_side * last + sign * (1 + 2 * inner))

    def row_scale(k):
        for c in range(2):
            e = 2 * chips[k] + c

            def wait(e=e):
                remote(rs_out.at[0], rs_in.at[e], rs_s.at[0], rs_r.at[e], sp=me).wait_recv()

            if k > 0:
                wait()
            else:
                pl.when(c != mi)(wait)
        return upright(rs_in[2 * chips[k]] + rs_in[2 * chips[k] + 1])[:, 0:1]

    depth = wg.shape[1]
    tile = min(256, depth)

    def expert_up(k):
        scale = row_scale(k)

        def up(n, carry):
            at = pl.ds(pl.multiple_of(n * tile, tile), tile)
            g = jnp.zeros((grp, tile), F32)
            u = jnp.zeros((grp, tile), F32)
            for b in range(ntp):
                x = arr[b, rows_of(k), :]
                g = g + dot(x, wg[b * ch:(b + 1) * ch, at])
                u = u + dot(x, wu[b * ch:(b + 1) * ch, at])
            hid[:, at] = (jax.nn.silu(g * scale) * (u * scale)).astype(BF16)
            return carry

        if k == 0:
            loads[1].wait()
            loads[2].wait()
        lax.fori_loop(0, depth // tile, up, 0)

    def expert_down(k):
        def down(b):
            at = pl.ds(pl.multiple_of(b * ch, ch), ch)
            part[b, rows_of(k), :] = dot(hid[...], wd[:, at]).astype(BF16)

        if k == 0:
            loads[3].wait()
        down(td)
        if k > 0:
            first(k, 1, td, 0, tx)
            first(k, 3, td, 1, ty)
        down(tx)
        if k > 0:
            first(k, 0, tx, 0, tx)
        down(ty)
        if k > 0:
            first(k, 2, ty, 1, ty)
        down(t)

    def first(k, n, of, c, to):
        send(remote(part.at[of, half(k, c)], one.at[n % 2, half(k, c)], r_s.at[6 * k + n],
                    r_r.at[6 * k + n], tp=to))

    def reduce_own(k):
        first(k, 1, td, 0, tx)
        first(k, 3, td, 1, ty)
        first(k, 0, tx, 0, tx)
        first(k, 2, ty, 1, ty)

    def summed(m, block):
        remote(block, block, r_s.at[m], r_r.at[m], tp=tx).wait_recv()

    def reduce_mid(k):
        n = 6 * k
        for c, to in ((0, ty), (1, tx)):
            at = half(k, c)
            summed(n + 1 + 2 * c, one.at[1, at])
            two_out[at, :] = (part[to, at, :].astype(F32) + one[1, at, :].astype(F32)).astype(BF16)
            m = n + 4 + c
            send(remote(two_out.at[at], two.at[at], r_s.at[m], r_r.at[m], tp=to))

    def reduce_end(k):
        n = 6 * k
        for c in range(2):
            at = half(k, c)
            summed(n + 2 * c, one.at[0, at])
            summed(n + 4 + c, two.at[at])
            fin[at, :] = (
                part[t, at, :].astype(F32) + one[0, at, :].astype(F32) + two[at, :].astype(F32)
            ).astype(BF16)
            e = 2 * chips[k] + c
            if k > 0:
                send(remote(fin.at[at], ret.at[piece(me)], h_s.at[e], h_r.at[me], sp=e))
        if k == 0:
            send(remote(fin.at[piece(sib)], ret.at[piece(me)], h_s.at[sib], h_r.at[me], sp=sib))
            ret[piece(me), :] = fin[piece(me), :]

    order = [
        (share, 0), (scales, 0), (relay, 0), (share, 1), (dispatch_last, 3), (gather_end, 0),
        (expert_up, 0), (relay, 1), (expert_down, 0), (share, 2), (gather_end, 1), (share, 3),
        (expert_up, 1), (relay, 2), (expert_down, 1), (relay, 3), (gather_end, 2),
        (expert_up, 2), (reduce_mid, 1), (expert_down, 2), (reduce_end, 1), (gather_end, 3),
        (expert_up, 3), (reduce_mid, 2), (expert_down, 3), (reduce_own, 0), (reduce_end, 2),
        (reduce_mid, 3), (reduce_mid, 0), (reduce_end, 3), (reduce_end, 0),
    ]
    for step, k in order:
        with jax.named_scope(step.__name__ + str(k)):
            step(k)

    with jax.named_scope("ret"):
        for d in range(1, nsp):
            e = (me + d) % nsp
            remote(fin.at[piece(0)], ret.at[piece(e)], h_s.at[0], h_r.at[e], sp=me).wait_recv()
    with jax.named_scope("final"):
        back = ret[...]
        moe = dot(pick0, back) * weights[:, 0:1] + dot(pick1, back) * weights[:, 1:2]
        out_ref[...] = (mixed[...] + moe).astype(out_ref.dtype)

    @pl.when(me < nsp - 1)
    def _():
        to_right.wait_send()

    @pl.when(me > 0)
    def _():
        to_left.wait_send()

    for d in range(1, nsp):
        e = (me + d) % nsp
        remote(outgoing.at[piece(e)], arr.at[t, piece(me)], zs_s.at[e], zs_r.at[me],
               sp=e).wait_send()
    for copy in pending:
        copy.wait_send()


def fused(nsp, ntp, *args):
    (residual, glu_value, glu_gate, conv_weight, conv_bias, ln_gain, ln_bias, out_weight,
     norm_gain, route_ids, route_weight, expert_gate, expert_up, expert_down) = args
    rows, ch = residual.shape
    width = out_weight.shape[0]
    depth = expert_gate.shape[2]
    cap = 2 * rows * TOPK // nsp
    slots = nsp * cap
    grp = 2 * cap
    edge = -(-(conv_weight.shape[0] // 2) // 16) * 16
    small = [residual, glu_value, glu_gate, conv_weight]
    small += [a.reshape(1, ch) for a in (conv_bias, ln_gain, ln_bias, norm_gain)]
    small += [route_ids.T, route_weight.T]
    vmem = pl.BlockSpec(memory_space=pltpu.VMEM)
    hbm = pl.BlockSpec(memory_space=pl.ANY)
    dma = lambda n: pltpu.SemaphoreType.DMA((n,))
    return pl.pallas_call(
        functools.partial(layer_kernel, nsp, ntp),
        out_shape=jax.ShapeDtypeStruct((rows, ch), residual.dtype),
        in_specs=[hbm] * 14,
        out_specs=vmem,
        scratch_shapes=[pltpu.VMEM(a.shape, a.dtype) for a in small] + [
            pltpu.VMEM((width, ch), BF16),
            pltpu.VMEM((width, depth), BF16),
            pltpu.VMEM((width, depth), BF16),
            pltpu.VMEM((depth, width), BF16),
            pltpu.VMEM((rows + 2 * edge, ch), F32),
            pltpu.VMEM((-(-conv_weight.shape[0] // 8) * 8, ch), F32),
            pltpu.VMEM((rows, ch), F32),
            pltpu.VMEM((rows, ch), F32),
            pltpu.VMEM((2, edge, ch), BF16),
            pltpu.VMEM((2, edge, ch), BF16),
            pltpu.VMEM((2, 8, rows), F32),
            pltpu.VMEM((2, ntp, 8, rows), F32),
            pltpu.VMEM((ntp, 1, ch), F32),
            pltpu.VMEM((ntp, 1, ch), F32),
            pltpu.VMEM((ntp, rows, ch), BF16),
            pltpu.VMEM((slots, ch), BF16),
            pltpu.VMEM((ntp, slots, ch), BF16),
            pltpu.VMEM((grp, depth), BF16),
            pltpu.VMEM((ntp, slots, ch), BF16),
            pltpu.VMEM((2, slots, ch), BF16),
            pltpu.VMEM((slots, ch), BF16),
            pltpu.VMEM((slots, ch), BF16),
            pltpu.VMEM((slots, ch), BF16),
            pltpu.VMEM((slots, ch), BF16),
            pltpu.VMEM((nsp, 8, grp), F32),
            pltpu.VMEM((nsp, 8, grp), F32),
            dma(14), dma(2), dma(2), dma(2 * ntp), dma(2 * ntp), dma(2 * ntp), dma(2 * ntp),
            dma(12), dma(12), dma(nsp), dma(nsp), dma(nsp), dma(nsp), dma(6 * GROUPS),
            dma(6 * GROUPS), dma(6 * GROUPS), dma(6 * GROUPS), dma(nsp), dma(nsp),
        ],
        compiler_params=pltpu.CompilerParams(
            collective_id=0, has_side_effects=True, vmem_limit_bytes=VMEM_LIMIT
        ),
    )(*small, out_weight, expert_gate, expert_up, expert_down)


def solution(mesh):
    in_specs = (
        P("sp", "tp"),
        P("sp", "tp"),
        P("sp", "tp"),
        P(None, "tp"),
        P("tp"),
        P("tp"),
        P("tp"),
        P(None, "tp"),
        P("tp"),
        P("sp", None),
        P("sp", None),
        P("sp", None, "tp"),
        P("sp", None, "tp"),
        P("sp", "tp", None),
    )
    out_specs = P("sp", "tp")
    nsp, ntp = mesh.shape["sp"], mesh.shape["tp"]
    body = on_device
    if ntp == 4 and nsp == 2 * GROUPS:
        body = functools.partial(fused, nsp, ntp)
    return jax.shard_map(
        body, mesh=mesh, in_specs=in_specs, out_specs=out_specs, check_vma=False
    )
```

time: 73.4 us -> 65.6 us (0.89)
  Pallas kernels: 71.7 us -> 63.7 us
    pallas_call x1, Pallas kernels: 71.7 us -> 63.7 us  [fused(): pl.pallas_call(functools.partial(layer_kernel, nsp, ntp), out_shape=jax.S...]
where the time goes in v1:
time: 65.6 us; the launch traced here: 65.3 us
  Pallas kernels  63.7 us (97%)
  local copies, waits for them, and re-layouts  1.57 us (2%)
    pallas_call x1, Pallas kernels, fused(): pl.pallas_call(functools.partial(layer_kernel, nsp, ntp), out_shape=jax.S...  63.7 us
    unnamed x1, local copies, waits for them, and re-layouts  1.57 us

profile of v1, /device:TPU:0, one launch (start us, length us, event | category | flops | bytes accessed | tf_op | source)
XLA Modules:
  0.0 65.3 jit_solution(12514516041110183925)
XLA Ops:
  0.0 63.7 %shard_map.136 = bf16[128,512]{1,0:T(8,128)(2,1)} custom-call(bf16[128,512]{1,0:T(8,128)(2,1)} %res_hbm.1, bf16[128,512]{1,0:T(8,128)(2,1)} %val_hbm.1, bf16[128,512]{1,0:T(8,128)(2,1)} %gate_hbm.1, bf16[31,512]{1,0:T(8,128)(2,1)} %cw_hbm.1, f32[1,512]{1,0:T(1,128)} %bitcast.6, f32[1,512]{1,0:T(1,128)} %bitcast.7, f32[1,512]{1,0:T(1,128)} %bitcast.8, ...), custom_call_target="tpu_custom_call" | custom-call | tf_op jit(solution)/shard_map/pallas_call | solution.py:607
  63.7 1.6 %copy.16 = bf16[128,512]{1,0:T(8,128)(2,1)} copy(bf16[128,512]{1,0:T(8,128)(2,1)} %shard_map.136) | data formatting | bytes 262144

commit v2 on v1

--- a/solution.py
+++ b/solution.py
@@ -207,16 +207,19 @@
     def _():
         to_left.start()
 
-    pending = []
-
     def send(copy):
         copy.start()
-        pending.append(copy)
+
+    def drain(ref, sem):
+        remote(ref, ref, sem, sem, tp=tx).wait_send()
+
+    def receive(ref, sem):
+        remote(ref, ref, sem, sem, tp=tx).wait_recv()
 
     others = (tx, ty, td)
-    for n, to in enumerate(others):
-        send(remote(lg_ref, lg_all.at[t], ln_s.at[n], ln_r.at[t], tp=to))
-        send(remote(lb_ref, lb_all.at[t], ln_s.at[ntp + n], ln_r.at[ntp + t], tp=to))
+    for to in others:
+        send(remote(lg_ref, lg_all.at[t], ln_s.at[0], ln_r.at[0], tp=to))
+        send(remote(lb_ref, lb_all.at[t], ln_s.at[1], ln_r.at[1], tp=to))
 
     def convolve(low, high):
         for j in range(0, ch, 128):
@@ -251,15 +254,12 @@
         for n, s in enumerate(sums):
             block = jnp.where(lane == n, s, block)
         st_out[which] = block.T[0:8, :]
-        for n, to in enumerate(others):
-            k = which * ntp
-            send(remote(st_out.at[which], st_in.at[which, t], st_s.at[k + n], st_r.at[k + t],
-                        tp=to))
-
-    def totals_of(which, b):
-        ref = st_in.at[which, b]
-        remote(st_out.at[which], ref, st_s.at[0], st_r.at[which * ntp + b], tp=tx).wait_recv()
-        return st_in[which, b]
+        for to in others:
+            send(remote(st_out.at[which], st_in.at[which, t], st_s.at[0], st_r.at[which], tp=to))
+
+    def totals(which):
+        receive(st_in.at[which, pl.ds(0, ntp - 1)], st_r.at[which])
+        return [st_out[which]] + [st_in[which, b] for b in others]
 
     def upright(block):
         fill = jnp.zeros((128 - block.shape[0], block.shape[1]), F32)
@@ -275,18 +275,13 @@
         s1 = jnp.sum(c, axis=1, keepdims=True)
         c = c - s1 / ch
         cc[t] = c.astype(BF16)
+        send_totals(0, (s1, jnp.sum(c * c, axis=1, keepdims=True)))
         for q in (0, 1, 2, 3):
             block = quarter(t, q)
-            send(remote(block, block, ag_s.at[q], ag_r.at[2 * q + q % 2], tp=(tx, ty)[q % 2]))
-        send_totals(0, (s1, jnp.sum(c * c, axis=1, keepdims=True)))
+            send(remote(block, block, ag_s.at[0], ag_r.at[q], tp=(tx, ty)[q % 2]))
         for q in (1, 0, 3, 2):
             block = quarter(t, q)
-            send(remote(block, block, ag_s.at[4 + q], ag_r.at[2 * q + 1 - q % 2],
-                        tp=(ty, tx)[q % 2]))
-
-    def arrived(of, q, n):
-        block = quarter(of, q)
-        remote(block, block, ag_s.at[0], ag_r.at[n], tp=tx).wait_recv()
+            send(remote(block, block, ag_s.at[0], ag_r.at[5 - q % 2], tp=(ty, tx)[q % 2]))
 
     with jax.named_scope("routes"):
         row = lax.broadcasted_iota(jnp.int32, (rows, rows), 0)
@@ -313,10 +308,10 @@
         pick_r = jnp.where(wide == lead0, 1.0, jnp.where(wide == lead1, 1.0, 0.0)).astype(BF16)
 
     def relay_ag(q):
-        of, n, to = ((tx, 2 * q, ty), (ty, 2 * q + 1, tx))[q % 2]
-        arrived(of, q, n)
+        of, to = ((tx, ty), (ty, tx))[q % 2]
         block = quarter(of, q)
-        send(remote(block, block, ag_s.at[8 + q], ag_r.at[8 + q], tp=to))
+        receive(block, ag_r.at[q])
+        send(remote(block, block, ag_s.at[0], ag_r.at[6], tp=to))
 
     def columns(of):
         return ow[pl.ds(pl.multiple_of(of * ch, ch), ch), :]
@@ -324,10 +319,15 @@
     with jax.named_scope("relay_a"):
         relay_ag(0)
         relay_ag(1)
+    with jax.named_scope("relay_b"):
+        relay_ag(2)
+        relay_ag(3)
+        receive(lg_all.at[pl.ds(0, ntp - 1)], ln_r.at[0])
+        receive(lb_all.at[pl.ds(0, ntp - 1)], ln_r.at[1])
     with jax.named_scope("ln_stats"):
         lg_all[t] = lg_ref[...]
         lb_all[t] = lb_ref[...]
-        stats = [st_out[0]] + [totals_of(0, b) for b in others]
+        stats = totals(0)
         total = stats[0] + stats[1] + stats[2] + stats[3]
         mean = total[0:1] / width
         offs = [s[0:1] / ch - mean for s in stats]
@@ -344,23 +344,14 @@
     with jax.named_scope("proj_own"):
         loads[0].wait()
         mixed[...] = res_ref[...].astype(F32) + project(t, 1)
-    with jax.named_scope("relay_b"):
-        relay_ag(2)
-        relay_ag(3)
-        for n, b in enumerate(others):
-            remote(lg_ref, lg_all.at[b], ln_s.at[0], ln_r.at[b], tp=tx).wait_recv()
-            remote(lb_ref, lb_all.at[b], ln_s.at[0], ln_r.at[ntp + b], tp=tx).wait_recv()
     with jax.named_scope("proj_x"):
-        arrived(tx, 1, 2)
-        arrived(tx, 3, 6)
+        receive(cc.at[tx, pl.ds(0, 2 * quart)], ag_r.at[4])
         mixed[...] += project(tx, 2)
     with jax.named_scope("proj_y"):
-        arrived(ty, 0, 1)
-        arrived(ty, 2, 5)
+        receive(cc.at[ty, pl.ds(0, 2 * quart)], ag_r.at[5])
         mixed[...] += project(ty, 3)
     with jax.named_scope("proj_d"):
-        for q in range(4):
-            arrived(td, q, 8 + q)
+        receive(cc.at[td], ag_r.at[6])
         full = mixed[...] + project(td, 4)
         mixed[...] = full
     with jax.named_scope("pick"):
@@ -371,7 +362,7 @@
         return pl.ds(pl.multiple_of(n * cap, cap), cap)
 
     def dispatch(e):
-        remote(outgoing.at[piece(e)], arr.at[t, piece(me)], zs_s.at[e], zs_r.at[me], sp=e).start()
+        remote(outgoing.at[piece(e)], arr.at[t, piece(me)], zs_s.at[0], zs_r.at[me], sp=e).start()
 
     def dispatch_chip(c):
         dispatch(2 * c + mi)
@@ -399,46 +390,29 @@
 
     def pass_on(k, n, of, at, to):
         block = arr.at[of, at]
-        send(remote(block, block, x_s.at[6 * k + n], x_r.at[6 * k + n], tp=to))
-
-    def landed(k, n, of, at):
-        block = arr.at[of, at]
-        remote(block, block, x_s.at[6 * k + n], x_r.at[6 * k + n], tp=tx).wait_recv()
-
-    def came(e):
-        remote(outgoing.at[piece(0)], arr.at[t, piece(e)], zs_s.at[0], zs_r.at[e],
-               sp=me).wait_recv()
+        send(remote(block, block, x_s.at[0], x_r.at[3 * k + n], tp=to))
 
     def share(k):
-        if k == 0:
-            pass_on(0, 2 * mi, t, piece(me), tx)
-            pass_on(0, 2 * mi + 1, t, piece(me), ty)
-            came(sib)
-            pass_on(0, 2 * (1 - mi), t, piece(sib), tx)
-            pass_on(0, 2 * (1 - mi) + 1, t, piece(sib), ty)
-            return
-        came(2 * chips[k])
-        came(2 * chips[k] + 1)
-        pass_on(k, 0, t, half(k, 0), tx)
-        pass_on(k, 3, t, half(k, 1), ty)
-        pass_on(k, 2, t, half(k, 1), tx)
-        pass_on(k, 1, t, half(k, 0), ty)
+        for c in (mi, 1 - mi) if k == 0 else (1, 0):
+            e = 2 * chips[k] + c
+            if k > 0:
+                receive(arr.at[t, piece(e)], zs_r.at[e])
+            elif c is not mi:
+                receive(arr.at[t, piece(e)], zs_r.at[e])
+            pass_on(k, 2 * c, t, piece(e), tx)
+            pass_on(k, 2 - c, t, piece(e), ty)
 
     def relay(k):
-        landed(k, 0, tx, half(k, 0))
-        pass_on(k, 4, tx, half(k, 0), ty)
-        landed(k, 3, ty, half(k, 1))
-        pass_on(k, 5, ty, half(k, 1), tx)
+        receive(arr.at[tx, half(k, 0)], x_r.at[3 * k])
+        pass_on(k, 2, tx, half(k, 0), ty)
+        receive(arr.at[ty, half(k, 1)], x_r.at[3 * k + 1])
+        pass_on(k, 2, ty, half(k, 1), tx)
 
     def gather_end(k):
-        landed(k, 1, ty, half(k, 0))
-        landed(k, 2, tx, half(k, 1))
-        landed(k, 4, td, half(k, 0))
-        landed(k, 5, td, half(k, 1))
+        receive(arr.at[0, pl.ds(0, 4 * cap)], x_r.at[3 * k + 2])
 
     def scales(k):
-        r = lax.rsqrt((st_out[1] + totals_of(1, tx) + totals_of(1, ty) + totals_of(1, td)) / width
-                      + 1e-06)[0:1]
+        r = lax.rsqrt(sum(totals(1)) / width + 1e-06)[0:1]
         top = r.astype(BF16).astype(F32)
         mid = (r - top).astype(BF16).astype(F32)
         low = r - top - mid
@@ -449,7 +423,7 @@
             rs_out[e] = jnp.broadcast_to(picked[:, e * grp:(e + 1) * grp], (8, grp))
         for d in range(1, nsp):
             e = (me + d) % nsp
-            send(remote(rs_out.at[e], rs_in.at[me], rs_s.at[e], rs_r.at[me], sp=e))
+            send(remote(rs_out.at[e], rs_in.at[me], rs_s.at[0], rs_r.at[z], sp=e))
         rs_in[me] = rs_out[me]
 
         @pl.when(inner == 0)
@@ -460,16 +434,7 @@
         dispatch_chip(far_side * last + sign * (1 + 2 * inner))
 
     def row_scale(k):
-        for c in range(2):
-            e = 2 * chips[k] + c
-
-            def wait(e=e):
-                remote(rs_out.at[0], rs_in.at[e], rs_s.at[0], rs_r.at[e], sp=me).wait_recv()
-
-            if k > 0:
-                wait()
-            else:
-                pl.when(c != mi)(wait)
+        receive(rs_in.at[pl.ds(0, 2 if k else 1)], rs_r.at[chips[k]])
         return upright(rs_in[2 * chips[k]] + rs_in[2 * chips[k] + 1])[:, 0:1]
 
     depth = wg.shape[1]
@@ -514,78 +479,74 @@
         down(t)
 
     def first(k, n, of, c, to):
-        send(remote(part.at[of, half(k, c)], one.at[n % 2, half(k, c)], r_s.at[6 * k + n],
-                    r_r.at[6 * k + n], tp=to))
-
-    def reduce_own(k):
+        send(remote(part.at[of, half(k, c)], one.at[n % 2, half(k, c)], r_s.at[0],
+                    r_r.at[4 * k + 2 * (1 - n % 2) + c], tp=to))
+
+    def own_far(k):
         first(k, 1, td, 0, tx)
         first(k, 3, td, 1, ty)
+
+    def own_near(k):
         first(k, 0, tx, 0, tx)
         first(k, 2, ty, 1, ty)
 
-    def summed(m, block):
-        remote(block, block, r_s.at[m], r_r.at[m], tp=tx).wait_recv()
-
     def reduce_mid(k):
-        n = 6 * k
         for c, to in ((0, ty), (1, tx)):
             at = half(k, c)
-            summed(n + 1 + 2 * c, one.at[1, at])
+            receive(one.at[1, at], r_r.at[4 * k + c])
             two_out[at, :] = (part[to, at, :].astype(F32) + one[1, at, :].astype(F32)).astype(BF16)
-            m = n + 4 + c
-            send(remote(two_out.at[at], two.at[at], r_s.at[m], r_r.at[m], tp=to))
+            send(remote(two_out.at[at], two.at[at], r_s.at[0], r_r.at[4 * k + 2 + c], tp=to))
 
     def reduce_end(k):
-        n = 6 * k
         for c in range(2):
             at = half(k, c)
-            summed(n + 2 * c, one.at[0, at])
-            summed(n + 4 + c, two.at[at])
+            receive(one.at[0, rows_of(k)], r_r.at[4 * k + 2 + c])
             fin[at, :] = (
                 part[t, at, :].astype(F32) + one[0, at, :].astype(F32) + two[at, :].astype(F32)
             ).astype(BF16)
             e = 2 * chips[k] + c
             if k > 0:
-                send(remote(fin.at[at], ret.at[piece(me)], h_s.at[e], h_r.at[me], sp=e))
+                send(remote(fin.at[at], ret.at[piece(me)], h_s.at[0], h_r.at[0], sp=e))
         if k == 0:
-            send(remote(fin.at[piece(sib)], ret.at[piece(me)], h_s.at[sib], h_r.at[me], sp=sib))
+            send(remote(fin.at[piece(sib)], ret.at[piece(me)], h_s.at[0], h_r.at[0], sp=sib))
             ret[piece(me), :] = fin[piece(me), :]
 
     order = [
-        (share, 0), (scales, 0), (relay, 0), (share, 1), (dispatch_last, 3), (gather_end, 0),
+        (share, 0), (relay, 0), (scales, 0), (share, 1), (dispatch_last, 3), (gather_end, 0),
         (expert_up, 0), (relay, 1), (expert_down, 0), (share, 2), (gather_end, 1), (share, 3),
         (expert_up, 1), (relay, 2), (expert_down, 1), (relay, 3), (gather_end, 2),
-        (expert_up, 2), (reduce_mid, 1), (expert_down, 2), (reduce_end, 1), (gather_end, 3),
-        (expert_up, 3), (reduce_mid, 2), (expert_down, 3), (reduce_own, 0), (reduce_end, 2),
-        (reduce_mid, 3), (reduce_mid, 0), (reduce_end, 3), (reduce_end, 0),
+        (expert_up, 2), (reduce_mid, 1), (expert_down, 2), (gather_end, 3), (expert_up, 3),
+        (reduce_end, 1), (reduce_mid, 2), (expert_down, 3), (own_far, 0), (reduce_end, 2),
+        (reduce_mid, 3), (own_near, 0), (reduce_mid, 0), (reduce_end, 3), (reduce_end, 0),
     ]
     for step, k in order:
         with jax.named_scope(step.__name__ + str(k)):
             step(k)
 
+    with jax.named_scope("drain"):
+        @pl.when(me < nsp - 1)
+        def _():
+            to_right.wait_send()
+
+        @pl.when(me > 0)
+        def _():
+            to_left.wait_send()
+
+        drain(lg_all.at[pl.ds(0, ntp - 1)], ln_s.at[0])
+        drain(lb_all.at[pl.ds(0, ntp - 1)], ln_s.at[1])
+        drain(rs_out.at[pl.ds(0, 2 * (ntp - 1))], st_s.at[0])
+        drain(cc.at[pl.ds(0, 3)], ag_s.at[0])
+        drain(outgoing.at[pl.ds(0, (nsp - 1) * cap)], zs_s.at[0])
+        drain(rs_out.at[pl.ds(0, nsp - 1)], rs_s.at[0])
+        drain(arr.at[pl.ds(0, 3)], x_s.at[0])
+        drain(arr.at[pl.ds(0, 3)], r_s.at[0])
     with jax.named_scope("ret"):
-        for d in range(1, nsp):
-            e = (me + d) % nsp
-            remote(fin.at[piece(0)], ret.at[piece(e)], h_s.at[0], h_r.at[e], sp=me).wait_recv()
+        receive(ret.at[pl.ds(0, (nsp - 1) * cap)], h_r.at[0])
     with jax.named_scope("final"):
         back = ret[...]
         moe = dot(pick0, back) * weights[:, 0:1] + dot(pick1, back) * weights[:, 1:2]
         out_ref[...] = (mixed[...] + moe).astype(out_ref.dtype)
-
-    @pl.when(me < nsp - 1)
-    def _():
-        to_right.wait_send()
-
-    @pl.when(me > 0)
-    def _():
-        to_left.wait_send()
-
-    for d in range(1, nsp):
-        e = (me + d) % nsp
-        remote(outgoing.at[piece(e)], arr.at[t, piece(me)], zs_s.at[e], zs_r.at[me],
-               sp=e).wait_send()
-    for copy in pending:
-        copy.wait_send()
+        drain(ret.at[pl.ds(0, (nsp - 1) * cap)], h_s.at[0])
 
 
 def fused(nsp, ntp, *args):
@@ -636,9 +597,9 @@
             pltpu.VMEM((slots, ch), BF16),
             pltpu.VMEM((nsp, 8, grp), F32),
             pltpu.VMEM((nsp, 8, grp), F32),
-            dma(14), dma(2), dma(2), dma(2 * ntp), dma(2 * ntp), dma(2 * ntp), dma(2 * ntp),
-            dma(12), dma(12), dma(nsp), dma(nsp), dma(nsp), dma(nsp), dma(6 * GROUPS),
-            dma(6 * GROUPS), dma(6 * GROUPS), dma(6 * GROUPS), dma(nsp), dma(nsp),
+            dma(14), dma(2), dma(2), dma(1), dma(2), dma(2), dma(2), dma(1), dma(7),
+            dma(1), dma(nsp), dma(1), dma(GROUPS), dma(1), dma(3 * GROUPS), dma(1),
+            dma(4 * GROUPS), dma(1), dma(1),
         ],
         compiler_params=pltpu.CompilerParams(
             collective_id=0, has_side_effects=True, vmem_limit_bytes=VMEM_LIMIT

time: 65.6 us -> 60.7 us (0.925)
  Pallas kernels: 63.7 us -> 58.8 us
    pallas_call x1, Pallas kernels: 63.7 us -> 58.8 us  [fused(): pl.pallas_call(functools.partial(layer_kernel, nsp, ntp), out_shape=jax.S...]
where the time goes in v2:
time: 60.7 us; the launch traced here: 60.4 us
  Pallas kernels  58.8 us (97%)
  local copies, waits for them, and re-layouts  1.57 us (3%)
    pallas_call x1, Pallas kernels, fused(): pl.pallas_call(functools.partial(layer_kernel, nsp, ntp), out_shape=jax.S...  58.8 us
    unnamed x1, local copies, waits for them, and re-layouts  1.57 us

profile of v2, /device:TPU:0, one launch (start us, length us, event | category | flops | bytes accessed | tf_op | source)
XLA Modules:
  0.0 60.4 jit_solution(13208727345859128087)
XLA Ops:
  0.0 58.8 %shard_map.136 = bf16[128,512]{1,0:T(8,128)(2,1)} custom-call(bf16[128,512]{1,0:T(8,128)(2,1)} %res_hbm.1, bf16[128,512]{1,0:T(8,128)(2,1)} %val_hbm.1, bf16[128,512]{1,0:T(8,128)(2,1)} %gate_hbm.1, bf16[31,512]{1,0:T(8,128)(2,1)} %cw_hbm.1, f32[1,512]{1,0:T(1,128)} %bitcast.6, f32[1,512]{1,0:T(1,128)} %bitcast.7, f32[1,512]{1,0:T(1,128)} %bitcast.8, ...), custom_call_target="tpu_custom_call" | custom-call | tf_op jit(solution)/shard_map/pallas_call | solution.py:568
  58.8 1.6 %copy.16 = bf16[128,512]{1,0:T(8,128)(2,1)} copy(bf16[128,512]{1,0:T(8,128)(2,1)} %shard_map.136) | data formatting | bytes 262144

commit v3 on v2

--- a/solution.py
+++ b/solution.py
@@ -122,6 +122,7 @@
     res_ref, val_ref, gate_ref, cw_ref, cb_ref, lg_ref, lb_ref, ng_ref, ids_ref, rw_ref,
     ow, wg, wu, wd, pad, wf, conv, mixed, halo_out, halo_in, st_out, st_in, lg_all, lb_all,
     cc, outgoing, arr, hid, part, one, two_out, two, fin, ret, rs_out, rs_in,
+    tok, placed, near, whole,
     w_sem, halo_s, halo_r, st_s, st_r, ln_s, ln_r, ag_s, ag_r, zs_s, zs_r, rs_s, rs_r,
     x_s, x_r, r_s, r_r, h_s, h_r,
 ):
@@ -145,8 +146,8 @@
     sign = 1 - 2 * far_side
     chips = [
         z,
+        far_side * last + sign * last,
         far_side * last + sign * (1 + inner),
-        far_side * last + sign * last,
         far_side * last + sign * (2 - 2 * inner),
     ]
     sib = 2 * z + 1 - mi
@@ -300,7 +301,7 @@
         slot = lax.broadcasted_iota(jnp.int32, (rows, nsp * cap), 1)
         pick0 = jnp.where(slot == id0 * cap + rank0, 1.0, 0.0)
         pick1 = jnp.where(slot == id1 * cap + rank1, 1.0, 0.0)
-        placing = (pick0 + pick1).T.astype(BF16)
+        placed[...] = (pick0 + pick1).T.astype(BF16)
         pick0 = pick0.astype(BF16)
         pick1 = pick1.astype(BF16)
         wide = lax.broadcasted_iota(jnp.int32, (rows, nsp * grp), 1)
@@ -354,12 +355,20 @@
         receive(cc.at[td], ag_r.at[6])
         full = mixed[...] + project(td, 4)
         mixed[...] = full
-    with jax.named_scope("pick"):
-        sq = jnp.sum(full * full, axis=1, keepdims=True)
-        outgoing[...] = dot(placing, (full * ng_ref[...]).astype(BF16)).astype(BF16)
-
     def piece(n):
         return pl.ds(pl.multiple_of(n * cap, cap), cap)
+
+    def pass_on(k, n, block, to):
+        send(remote(block, block, x_s.at[0], x_r.at[5 * k + n], tp=to))
+
+    with jax.named_scope("pick"):
+        tok[t] = (full * ng_ref[...]).astype(BF16)
+        parts = [tok.at[t, pl.ds(q * quart, quart)] for q in range(4)]
+        for q in range(4):
+            pass_on(0, q, parts[q], (tx, ty)[q % 2])
+        for q in range(4):
+            pass_on(0, 4, parts[q ^ 1], (tx, ty)[q % 2])
+        outgoing[...] = dot(placed[...], tok[t]).astype(BF16)
 
     def dispatch(e):
         remote(outgoing.at[piece(e)], arr.at[t, piece(me)], zs_s.at[0], zs_r.at[me], sp=e).start()
@@ -368,19 +377,12 @@
         dispatch(2 * c + mi)
         dispatch(2 * c + 1 - mi)
 
-    def dispatch_pair():
+    last_chip = far_side * last + sign * (1 + 2 * inner)
+    with jax.named_scope("zsend"):
+        dispatch_chip(far_side * last + sign * (3 - 3 * inner))
         dispatch_chip(far_side * last + sign * 2)
-        dispatch_chip(far_side * last + sign * (3 - 3 * inner))
-
-    with jax.named_scope("zsend"):
-        dispatch(sib)
-
-        @pl.when(inner == 1)
-        def _():
-            dispatch_pair()
-
-        arr[t, piece(me), :] = outgoing[piece(me), :]
-        send_totals(1, (sq,))
+
+        send_totals(1, (jnp.sum(full * full, axis=1, keepdims=True),))
 
     def rows_of(k):
         return pl.ds(pl.multiple_of(chips[k] * grp, grp), grp)
@@ -388,28 +390,51 @@
     def half(k, c):
         return piece(2 * chips[k] + c)
 
-    def pass_on(k, n, of, at, to):
-        block = arr.at[of, at]
-        send(remote(block, block, x_s.at[0], x_r.at[3 * k + n], tp=to))
+    def way(k, of, q):
+        if k == 0:
+            return tok.at[of, pl.ds(q * quart, quart)]
+        start = 2 * chips[k] * cap + q * (cap // 2)
+        return arr.at[of, pl.ds(pl.multiple_of(start, cap // 2), cap // 2)]
 
     def share(k):
-        for c in (mi, 1 - mi) if k == 0 else (1, 0):
+        for c in (1, 0):
             e = 2 * chips[k] + c
-            if k > 0:
-                receive(arr.at[t, piece(e)], zs_r.at[e])
-            elif c is not mi:
-                receive(arr.at[t, piece(e)], zs_r.at[e])
-            pass_on(k, 2 * c, t, piece(e), tx)
-            pass_on(k, 2 - c, t, piece(e), ty)
+            receive(arr.at[t, piece(e)], zs_r.at[e])
+            one_way, other = way(k, t, 2 * c), way(k, t, 2 * c + 1)
+            pass_on(k, 2 * c, one_way, tx)
+            pass_on(k, 2 * c + 1, other, ty)
+            pass_on(k, 4, other, tx)
+            pass_on(k, 4, one_way, ty)
 
     def relay(k):
-        receive(arr.at[tx, half(k, 0)], x_r.at[3 * k])
-        pass_on(k, 2, tx, half(k, 0), ty)
-        receive(arr.at[ty, half(k, 1)], x_r.at[3 * k + 1])
-        pass_on(k, 2, ty, half(k, 1), tx)
+        for q in (2, 3, 0, 1) if k else (0, 1, 2, 3):
+            of, to = ((tx, ty), (ty, tx))[q % 2]
+            receive(way(k, of, q), x_r.at[5 * k + q])
+            pass_on(k, 4, way(k, of, q), to)
 
     def gather_end(k):
-        receive(arr.at[0, pl.ds(0, 4 * cap)], x_r.at[3 * k + 2])
+        if k < last:
+            receive(arr.at[0, pl.ds(0, 4 * cap)], x_r.at[5 * k + 4])
+            return
+        for c in (1, 0):
+            e = 2 * chips[k] + c
+            receive(arr.at[:, piece(e)], zs_r.at[e])
+
+    def place(k):
+        to = [me, sib, 2 * last_chip, 2 * last_chip + 1]
+        both = jnp.concatenate([placed[piece(e), :] for e in to], axis=0)
+        for b in range(ntp):
+            rows_b = dot(both, tok[b]).astype(BF16)
+            arr[b, piece(me), :] = rows_b[:cap]
+            near[b] = rows_b[cap:2 * cap]
+            whole[0, b] = rows_b[2 * cap:3 * cap]
+            whole[1, b] = rows_b[3 * cap:]
+        send(remote(near, arr.at[:, piece(me)], zs_s.at[1], zs_r.at[me], sp=sib))
+        for c in (0, 1):
+            send(remote(whole.at[c], arr.at[:, piece(me)], zs_s.at[2], zs_r.at[me], sp=to[2 + c]))
+
+    def sibling(k):
+        receive(arr.at[:, piece(sib)], zs_r.at[sib])
 
     def scales(k):
         r = lax.rsqrt(sum(totals(1)) / width + 1e-06)[0:1]
@@ -426,13 +451,6 @@
             send(remote(rs_out.at[e], rs_in.at[me], rs_s.at[0], rs_r.at[z], sp=e))
         rs_in[me] = rs_out[me]
 
-        @pl.when(inner == 0)
-        def _():
-            dispatch_pair()
-
-    def dispatch_last(k):
-        dispatch_chip(far_side * last + sign * (1 + 2 * inner))
-
     def row_scale(k):
         receive(rs_in.at[pl.ds(0, 2 if k else 1)], rs_r.at[chips[k]])
         return upright(rs_in[2 * chips[k]] + rs_in[2 * chips[k] + 1])[:, 0:1]
@@ -478,9 +496,18 @@
             first(k, 2, ty, 1, ty)
         down(t)
 
+    def sub(k, c, p):
+        start = (2 * chips[k] + c) * cap + p * (cap // 2)
+        return pl.ds(pl.multiple_of(start, cap // 2), cap // 2)
+
     def first(k, n, of, c, to):
-        send(remote(part.at[of, half(k, c)], one.at[n % 2, half(k, c)], r_s.at[0],
-                    r_r.at[4 * k + 2 * (1 - n % 2) + c], tp=to))
+        if n % 2:
+            for p in range(2):
+                send(remote(part.at[of, sub(k, c, p)], one.at[1, sub(k, c, p)], r_s.at[0],
+                            r_r.at[8 * k + 2 * p + c], tp=to))
+        else:
+            send(remote(part.at[of, half(k, c)], one.at[0, half(k, c)], r_s.at[0],
+                        r_r.at[8 * k + 4 + c], tp=to))
 
     def own_far(k):
         first(k, 1, td, 0, tx)
@@ -491,30 +518,40 @@
         first(k, 2, ty, 1, ty)
 
     def reduce_mid(k):
-        for c, to in ((0, ty), (1, tx)):
-            at = half(k, c)
-            receive(one.at[1, at], r_r.at[4 * k + c])
-            two_out[at, :] = (part[to, at, :].astype(F32) + one[1, at, :].astype(F32)).astype(BF16)
-            send(remote(two_out.at[at], two.at[at], r_s.at[0], r_r.at[4 * k + 2 + c], tp=to))
+        for p in range(2):
+            for c, to in ((0, ty), (1, tx)):
+                at = sub(k, c, p)
+                receive(one.at[1, at], r_r.at[8 * k + 2 * p + c])
+                two_out[at, :] = (part[to, at, :].astype(F32) + one[1, at, :].astype(F32)).astype(
+                    BF16
+                )
+                send(remote(two_out.at[at], two.at[at], r_s.at[0],
+                            r_r.at[8 * k + 4 + 2 * p + c], tp=to))
 
     def reduce_end(k):
-        for c in range(2):
-            at = half(k, c)
-            receive(one.at[0, rows_of(k)], r_r.at[4 * k + 2 + c])
-            fin[at, :] = (
-                part[t, at, :].astype(F32) + one[0, at, :].astype(F32) + two[at, :].astype(F32)
-            ).astype(BF16)
-            e = 2 * chips[k] + c
-            if k > 0:
-                send(remote(fin.at[at], ret.at[piece(me)], h_s.at[0], h_r.at[0], sp=e))
+        for p in range(2):
+            for c in range(2):
+                at = sub(k, c, p)
+                if p == 0:
+                    receive(one.at[0, pl.ds(0, cap + cap // 2)], r_r.at[8 * k + 4 + c])
+                else:
+                    receive(two.at[at], r_r.at[8 * k + 6 + c])
+                fin[at, :] = (
+                    part[t, at, :].astype(F32) + one[0, at, :].astype(F32)
+                    + two[at, :].astype(F32)
+                ).astype(BF16)
+                if k > 0:
+                    back = pl.ds(pl.multiple_of(me * cap + p * (cap // 2), cap // 2), cap // 2)
+                    send(remote(fin.at[at], ret.at[back], h_s.at[0], h_r.at[0],
+                                sp=2 * chips[k] + c))
         if k == 0:
             send(remote(fin.at[piece(sib)], ret.at[piece(me)], h_s.at[0], h_r.at[0], sp=sib))
             ret[piece(me), :] = fin[piece(me), :]
 
     order = [
-        (share, 0), (relay, 0), (scales, 0), (share, 1), (dispatch_last, 3), (gather_end, 0),
-        (expert_up, 0), (relay, 1), (expert_down, 0), (share, 2), (gather_end, 1), (share, 3),
-        (expert_up, 1), (relay, 2), (expert_down, 1), (relay, 3), (gather_end, 2),
+        (relay, 0), (share, 1), (gather_end, 0), (scales, 0), (place, 0), (share, 2), (relay, 1),
+        (sibling, 0), (expert_up, 0), (expert_down, 0), (gather_end, 1), (relay, 2),
+        (expert_up, 1), (expert_down, 1), (gather_end, 2),
         (expert_up, 2), (reduce_mid, 1), (expert_down, 2), (gather_end, 3), (expert_up, 3),
         (reduce_end, 1), (reduce_mid, 2), (expert_down, 3), (own_far, 0), (reduce_end, 2),
         (reduce_mid, 3), (own_near, 0), (reduce_mid, 0), (reduce_end, 3), (reduce_end, 0),
@@ -536,9 +573,11 @@
         drain(lb_all.at[pl.ds(0, ntp - 1)], ln_s.at[1])
         drain(rs_out.at[pl.ds(0, 2 * (ntp - 1))], st_s.at[0])
         drain(cc.at[pl.ds(0, 3)], ag_s.at[0])
-        drain(outgoing.at[pl.ds(0, (nsp - 1) * cap)], zs_s.at[0])
+        drain(outgoing.at[pl.ds(0, 4 * cap)], zs_s.at[0])
+        drain(whole, zs_s.at[2])
+        drain(near, zs_s.at[1])
         drain(rs_out.at[pl.ds(0, nsp - 1)], rs_s.at[0])
-        drain(arr.at[pl.ds(0, 3)], x_s.at[0])
+        drain(arr.at[pl.ds(0, 3), pl.ds(0, 6 * cap)], x_s.at[0])
         drain(arr.at[pl.ds(0, 3)], r_s.at[0])
     with jax.named_scope("ret"):
         receive(ret.at[pl.ds(0, (nsp - 1) * cap)], h_r.at[0])
@@ -597,9 +636,13 @@
             pltpu.VMEM((slots, ch), BF16),
             pltpu.VMEM((nsp, 8, grp), F32),
             pltpu.VMEM((nsp, 8, grp), F32),
+            pltpu.VMEM((ntp, rows, ch), BF16),
+            pltpu.VMEM((slots, rows), BF16),
+            pltpu.VMEM((ntp, cap, ch), BF16),
+            pltpu.VMEM((2, ntp, cap, ch), BF16),
             dma(14), dma(2), dma(2), dma(1), dma(2), dma(2), dma(2), dma(1), dma(7),
-            dma(1), dma(nsp), dma(1), dma(GROUPS), dma(1), dma(3 * GROUPS), dma(1),
-            dma(4 * GROUPS), dma(1), dma(1),
+            dma(3), dma(nsp), dma(1), dma(GROUPS), dma(1), dma(5 * GROUPS - 5), dma(1),
+            dma(8 * GROUPS), dma(1), dma(1),
         ],
         compiler_params=pltpu.CompilerParams(
             collective_id=0, has_side_effects=True, vmem_limit_bytes=VMEM_LIMIT

time: 60.7 us -> 55.5 us (0.914)
  Pallas kernels: 58.8 us -> 53.8 us
    pallas_call x1, Pallas kernels: 58.8 us -> 53.8 us  [fused(): pl.pallas_call(functools.partial(layer_kernel, nsp, ntp), out_shape=jax.S...]
where the time goes in v3:
time: 55.5 us; the launch traced here: 55.3 us
  Pallas kernels  53.8 us (97%)
  local copies, waits for them, and re-layouts  1.57 us (3%)
    pallas_call x1, Pallas kernels, fused(): pl.pallas_call(functools.partial(layer_kernel, nsp, ntp), out_shape=jax.S...  53.8 us
    unnamed x1, local copies, waits for them, and re-layouts  1.57 us

profile of v3, /device:TPU:0, one launch (start us, length us, event | category | flops | bytes accessed | tf_op | source)
XLA Modules:
  0.0 55.3 jit_solution(12852405705813498010)
XLA Ops:
  0.0 53.8 %shard_map.136 = bf16[128,512]{1,0:T(8,128)(2,1)} custom-call(bf16[128,512]{1,0:T(8,128)(2,1)} %res_hbm.1, bf16[128,512]{1,0:T(8,128)(2,1)} %val_hbm.1, bf16[128,512]{1,0:T(8,128)(2,1)} %gate_hbm.1, bf16[31,512]{1,0:T(8,128)(2,1)} %cw_hbm.1, f32[1,512]{1,0:T(1,128)} %bitcast.6, f32[1,512]{1,0:T(1,128)} %bitcast.7, f32[1,512]{1,0:T(1,128)} %bitcast.8, ...), custom_call_target="tpu_custom_call" | custom-call | tf_op jit(solution)/shard_map/pallas_call | solution.py:607
  53.8 1.6 %copy.16 = bf16[128,512]{1,0:T(8,128)(2,1)} copy(bf16[128,512]{1,0:T(8,128)(2,1)} %shard_map.136) | data formatting | bytes 262144

commit v4 on v3

--- a/solution.py
+++ b/solution.py
@@ -123,7 +123,7 @@
     ow, wg, wu, wd, pad, wf, conv, mixed, halo_out, halo_in, st_out, st_in, lg_all, lb_all,
     cc, outgoing, arr, hid, part, one, two_out, two, fin, ret, rs_out, rs_in,
     tok, placed, near, whole,
-    w_sem, halo_s, halo_r, st_s, st_r, ln_s, ln_r, ag_s, ag_r, zs_s, zs_r, rs_s, rs_r,
+    here, w_sem, halo_s, halo_r, st_s, st_r, ln_s, ln_r, ag_s, ag_r, zs_s, zs_r, rs_s, rs_r,
     x_s, x_r, r_s, r_r, h_s, h_r,
 ):
     rows, ch = res_ref.shape
@@ -167,12 +167,20 @@
     for load in staged:
         load.start()
     barrier = pltpu.get_barrier_semaphore()
-    for d in range(1, ntp):
-        pl.semaphore_signal(barrier, inc=1, device_id={"tp": (t + d) % ntp},
-                            device_id_type=pl.DeviceIdType.MESH)
-    for d in range(1, nsp):
-        pl.semaphore_signal(barrier, inc=1, device_id={"sp": (me + d) % nsp},
-                            device_id_type=pl.DeviceIdType.MESH)
+
+    def signal(sem, **dev):
+        pl.semaphore_signal(sem, inc=1, device_id=dev, device_id_type=pl.DeviceIdType.MESH)
+
+    def along(d, act):
+        pl.when(me >= d)(lambda: act(me - d))
+        pl.when(me < nsp - d)(lambda: act(me + d))
+
+    def present(d):
+        return (me + nsp - d) // nsp + (2 * nsp - 1 - d - me) // nsp
+
+    signal(barrier, tp=tx)
+    signal(barrier, tp=ty)
+    along(1, lambda e: signal(barrier, sp=e))
     loads = [
         pltpu.make_async_copy(ow_hbm, ow, w_sem.at[0]),
         pltpu.make_async_copy(eg_hbm.at[0], wg, w_sem.at[1]),
@@ -195,7 +203,7 @@
             load.wait()
         wf[0:taps, :] = cw_ref[...].astype(F32)
     with jax.named_scope("bar"):
-        pl.semaphore_wait(barrier, ntp + nsp - 2)
+        pl.semaphore_wait(barrier, 2 + present(1))
     to_right = remote(halo_out.at[0], halo_in.at[0], halo_s.at[0], halo_r.at[0], sp=(me + 1) % nsp)
     to_left = remote(halo_out.at[1], halo_in.at[1], halo_s.at[1], halo_r.at[1],
                      sp=(me + nsp - 1) % nsp)
@@ -218,9 +226,20 @@
         remote(ref, ref, sem, sem, tp=tx).wait_recv()
 
     others = (tx, ty, td)
-    for to in others:
+
+    def send_ln(to):
         send(remote(lg_ref, lg_all.at[t], ln_s.at[0], ln_r.at[0], tp=to))
         send(remote(lb_ref, lb_all.at[t], ln_s.at[1], ln_r.at[1], tp=to))
+
+    signal(here.at[0], tp=tx)
+    along(1, lambda e: signal(here.at[1], sp=e))
+    send_ln(tx)
+    send_ln(ty)
+
+    def heard(n):
+        pl.semaphore_wait(here.at[1 + n // 2], present(n))
+        if n < 4:
+            along(2 * n, lambda e: signal(here.at[1 + n], sp=e))
 
     def convolve(low, high):
         for j in range(0, ch, 128):
@@ -234,6 +253,9 @@
         convolve(edge, rows - edge)
 
     with jax.named_scope("halo"):
+        pl.semaphore_wait(here.at[0], 1)
+        send_ln(td)
+
         @pl.when(me > 0)
         def _():
             to_right.wait_recv()
@@ -243,6 +265,8 @@
         def _():
             to_left.wait_recv()
             pad[edge + rows:, :] = halo_in[1].astype(F32)
+
+        heard(1)
 
     with jax.named_scope("conv_edge"):
         convolve(0, edge)
@@ -320,6 +344,7 @@
     with jax.named_scope("relay_a"):
         relay_ag(0)
         relay_ag(1)
+        heard(2)
     with jax.named_scope("relay_b"):
         relay_ag(2)
         relay_ag(3)
@@ -351,6 +376,7 @@
     with jax.named_scope("proj_y"):
         receive(cc.at[ty, pl.ds(0, 2 * quart)], ag_r.at[5])
         mixed[...] += project(ty, 3)
+        heard(4)
     with jax.named_scope("proj_d"):
         receive(cc.at[td], ag_r.at[6])
         full = mixed[...] + project(td, 4)
@@ -477,24 +503,30 @@
             loads[2].wait()
         lax.fori_loop(0, depth // tile, up, 0)
 
-    def expert_down(k):
-        def down(b):
-            at = pl.ds(pl.multiple_of(b * ch, ch), ch)
-            part[b, rows_of(k), :] = dot(hid[...], wd[:, at]).astype(BF16)
-
+    def down(k, b):
+        at = pl.ds(pl.multiple_of(b * ch, ch), ch)
+        part[b, rows_of(k), :] = dot(hid[...], wd[:, at]).astype(BF16)
+
+    def down_far(k):
         if k == 0:
             loads[3].wait()
-        down(td)
+        down(k, td)
         if k > 0:
             first(k, 1, td, 0, tx)
             first(k, 3, td, 1, ty)
-        down(tx)
+
+    def down_rest(k):
+        down(k, tx)
         if k > 0:
             first(k, 0, tx, 0, tx)
-        down(ty)
+        down(k, ty)
         if k > 0:
             first(k, 2, ty, 1, ty)
-        down(t)
+        down(k, t)
+
+    def expert_down(k):
+        down_far(k)
+        down_rest(k)
 
     def sub(k, c, p):
         start = (2 * chips[k] + c) * cap + p * (cap // 2)
@@ -551,10 +583,10 @@
     order = [
         (relay, 0), (share, 1), (gather_end, 0), (scales, 0), (place, 0), (share, 2), (relay, 1),
         (sibling, 0), (expert_up, 0), (expert_down, 0), (gather_end, 1), (relay, 2),
-        (expert_up, 1), (expert_down, 1), (gather_end, 2),
+        (expert_up, 1), (expert_down, 1), (own_far, 0), (gather_end, 2),
         (expert_up, 2), (reduce_mid, 1), (expert_down, 2), (gather_end, 3), (expert_up, 3),
-        (reduce_end, 1), (reduce_mid, 2), (expert_down, 3), (own_far, 0), (reduce_end, 2),
-        (reduce_mid, 3), (own_near, 0), (reduce_mid, 0), (reduce_end, 3), (reduce_end, 0),
+        (down_far, 3), (reduce_end, 1), (reduce_mid, 2), (down_rest, 3), (reduce_mid, 3),
+        (own_near, 0), (reduce_mid, 0), (reduce_end, 2), (reduce_end, 3), (reduce_end, 0),
     ]
     for step, k in order:
         with jax.named_scope(step.__name__ + str(k)):
@@ -640,7 +672,7 @@
             pltpu.VMEM((slots, rows), BF16),
             pltpu.VMEM((ntp, cap, ch), BF16),
             pltpu.VMEM((2, ntp, cap, ch), BF16),
-            dma(14), dma(2), dma(2), dma(1), dma(2), dma(2), dma(2), dma(1), dma(7),
+            pltpu.SemaphoreType.REGULAR((4,)), dma(14), dma(2), dma(2), dma(1), dma(2), dma(2), dma(2), dma(1), dma(7),
             dma(3), dma(nsp), dma(1), dma(GROUPS), dma(1), dma(5 * GROUPS - 5), dma(1),
             dma(8 * GROUPS), dma(1), dma(1),
         ],

time: 55.5 us -> 54.7 us (0.986)
  Pallas kernels: 53.8 us -> 53 us
    pallas_call x1, Pallas kernels: 53.8 us -> 53 us  [fused(): pl.pallas_call(functools.partial(layer_kernel, nsp, ntp), out_shape=jax.S...]
where the time goes in v4:
time: 54.7 us; the launch traced here: 54.6 us
  Pallas kernels  53 us (97%)
  local copies, waits for them, and re-layouts  1.57 us (3%)
    pallas_call x1, Pallas kernels, fused(): pl.pallas_call(functools.partial(layer_kernel, nsp, ntp), out_shape=jax.S...  53 us
    unnamed x1, local copies, waits for them, and re-layouts  1.57 us

profile of v4, /device:TPU:0, one launch (start us, length us, event | category | flops | bytes accessed | tf_op | source)
XLA Modules:
  0.0 54.6 jit_solution(15111129411048299146)
XLA Ops:
  0.0 53.0 %shard_map.136 = bf16[128,512]{1,0:T(8,128)(2,1)} custom-call(bf16[128,512]{1,0:T(8,128)(2,1)} %res_hbm.1, bf16[128,512]{1,0:T(8,128)(2,1)} %val_hbm.1, bf16[128,512]{1,0:T(8,128)(2,1)} %gate_hbm.1, bf16[31,512]{1,0:T(8,128)(2,1)} %cw_hbm.1, f32[1,512]{1,0:T(1,128)} %bitcast.6, f32[1,512]{1,0:T(1,128)} %bitcast.7, f32[1,512]{1,0:T(1,128)} %bitcast.8, ...), custom_call_target="tpu_custom_call" | custom-call | tf_op jit(solution)/shard_map/pallas_call | solution.py:639
  53.0 1.6 %copy.16 = bf16[128,512]{1,0:T(8,128)(2,1)} copy(bf16[128,512]{1,0:T(8,128)(2,1)} %shard_map.136) | data formatting | bytes 262144

commit v5 on v4

--- a/solution.py
+++ b/solution.py
@@ -422,8 +422,8 @@
         start = 2 * chips[k] * cap + q * (cap // 2)
         return arr.at[of, pl.ds(pl.multiple_of(start, cap // 2), cap // 2)]
 
-    def share(k):
-        for c in (1, 0):
+    def share(k, cores=(1, 0)):
+        for c in cores:
             e = 2 * chips[k] + c
             receive(arr.at[t, piece(e)], zs_r.at[e])
             one_way, other = way(k, t, 2 * c), way(k, t, 2 * c + 1)
@@ -431,6 +431,12 @@
             pass_on(k, 2 * c + 1, other, ty)
             pass_on(k, 4, other, tx)
             pass_on(k, 4, one_way, ty)
+
+    def share_one(k):
+        share(k, (1,))
+
+    def share_zero(k):
+        share(k, (0,))
 
     def relay(k):
         for q in (2, 3, 0, 1) if k else (0, 1, 2, 3):
@@ -581,7 +587,7 @@
             ret[piece(me), :] = fin[piece(me), :]
 
     order = [
-        (relay, 0), (share, 1), (gather_end, 0), (scales, 0), (place, 0), (share, 2), (relay, 1),
+        (relay, 0), (share, 1), (gather_end, 0), (scales, 0), (place, 0), (share_one, 2), (relay, 1), (share_zero, 2),
         (sibling, 0), (expert_up, 0), (expert_down, 0), (gather_end, 1), (relay, 2),
         (expert_up, 1), (expert_down, 1), (own_far, 0), (gather_end, 2),
         (expert_up, 2), (reduce_mid, 1), (expert_down, 2), (gather_end, 3), (expert_up, 3),

time: 54.7 us -> 53.8 us (0.984)
  Pallas kernels: 53 us -> 52.1 us
    pallas_call x1, Pallas kernels: 53 us -> 52.1 us  [fused(): pl.pallas_call(functools.partial(layer_kernel, nsp, ntp), out_shape=jax.S...]
where the time goes in v5:
time: 53.8 us; the launch traced here: 53.7 us
  Pallas kernels  52.1 us (97%)
  local copies, waits for them, and re-layouts  1.57 us (3%)
    pallas_call x1, Pallas kernels, fused(): pl.pallas_call(functools.partial(layer_kernel, nsp, ntp), out_shape=jax.S...  52.1 us
    unnamed x1, local copies, waits for them, and re-layouts  1.57 us

profile of v5, /device:TPU:0, one launch (start us, length us, event | category | flops | bytes accessed | tf_op | source)
XLA Modules:
  0.0 53.7 jit_solution(2663950633747369169)
XLA Ops:
  0.0 52.1 %shard_map.136 = bf16[128,512]{1,0:T(8,128)(2,1)} custom-call(bf16[128,512]{1,0:T(8,128)(2,1)} %res_hbm.1, bf16[128,512]{1,0:T(8,128)(2,1)} %val_hbm.1, bf16[128,512]{1,0:T(8,128)(2,1)} %gate_hbm.1, bf16[31,512]{1,0:T(8,128)(2,1)} %cw_hbm.1, f32[1,512]{1,0:T(1,128)} %bitcast.6, f32[1,512]{1,0:T(1,128)} %bitcast.7, f32[1,512]{1,0:T(1,128)} %bitcast.8, ...), custom_call_target="tpu_custom_call" | custom-call | tf_op jit(solution)/shard_map/pallas_call | solution.py:645
  52.1 1.6 %copy.16 = bf16[128,512]{1,0:T(8,128)(2,1)} copy(bf16[128,512]{1,0:T(8,128)(2,1)} %shard_map.136) | data formatting | bytes 262144
